TPU v7x, 128 devices: a whole 4x4x4 slice. The times are simulated.
128 devices in a mesh: sp: 32 (over z, y, core), tp: 4 (over x).
Axes of the slice: x: 4, y: 4, z: 4, core: 2. Of those that a mesh axis runs over, the one named last changes fastest.
Arguments:
- queries: bfloat16 [16384, 2048], P('sp', 'tp'), may hold values from -8 to 8
- keys: bfloat16 [16384, 512], P('sp', 'tp'), may hold values from -8 to 8
- values: bfloat16 [16384, 512], P('sp', 'tp'), may hold values from -6 to 6
- q_gain: float32 [128], replicated, may hold values from 0.1 to 5.8
- k_gain: float32 [128], replicated, may hold values from 0.1 to 5.8
- out_weight: bfloat16 [2048, 2048], replicated, may hold values from -0.125 to 0.125
- out_gain: float32 [2048], replicated, may hold values from 0.1 to 1.9
- residual_in: bfloat16 [16384, 2048], P(('sp', 'tp')), may hold values from -6 to 6
- mlp_gain: float32 [2048], replicated, may hold values from 0.1 to 1.9
- gate_weight: bfloat16 [2048, 5632], P('sp', 'tp'), may hold values from -0.125 to 0.125
- up_weight: bfloat16 [2048, 5632], P('sp', 'tp'), may hold values from -0.125 to 0.125
- down_weight: bfloat16 [5632, 2048], P('tp', 'sp'), may hold values from -0.078125 to 0.078125
- final_gain: float32 [2048], replicated, may hold values from 0.1 to 1.9
Outputs:
- layer_out: bfloat16 [16384, 2048], P(('sp', 'tp'))
All inputs are finite; a program needn't handle non-finite values.
Results may differ from a plain program's by a relative error of at most 0.015.
The roundings to bfloat16 on the way count: a program that leaves them out, or rounds other values in their place, can miss the bound.
Values may be sent and summed in bfloat16 or wider, within the bound.
A program may use at most 128 MiB of HBM per device.

v0:
```python
import math

import jax
import jax.numpy as jnp
from jax import lax
from jax.sharding import PartitionSpec as P

GRID_W = 64


def in_one_piece(arrays, axis, dim, along):
    ends, at = ([], 0)
    for a in arrays[:-1]:
        at += a.shape[along]
        ends.append(at)
    both = jnp.concatenate(arrays, axis=along)
    return tuple(jnp.split(lax.all_gather(both, axis, axis=dim, tiled=True), ends, axis=along))


def joined_along(pieces, dim):
    dims = list(pieces.shape[1:])
    dims[dim] *= pieces.shape[0]
    return jnp.moveaxis(pieces, 0, dim).reshape(dims)


def copy_for_each(array, axis):
    copies = jnp.broadcast_to(array, (lax.axis_size(axis), *array.shape))
    return lax.all_to_all(copies, axis, split_axis=0, concat_axis=0, tiled=True)


def gather_directly(array, axis, dim):
    return joined_along(copy_for_each(array, axis), dim)


def split_up(array, dim, length):
    before, after = (array.shape[:dim], array.shape[dim + 1 :])
    return jnp.moveaxis(array.reshape(*before, length, -1, *after), dim, 0)


def sum_at_owner(array, axis, dim):
    pieces = split_up(array, dim, lax.axis_size(axis))
    arrived = lax.all_to_all(pieces, axis, split_axis=0, concat_axis=0, tiled=True)
    return arrived.astype(jnp.float32).sum(axis=0)


def rms_scale(matrix):
    return matrix * lax.rsqrt(jnp.mean(matrix * matrix, axis=-1, keepdims=True) + 1e-06)


def rotary(matrix, positions):
    quarter = matrix.shape[-1] // 4
    freqs = 10000.0 ** (-jnp.arange(quarter, dtype=jnp.float32) / quarter)
    grid = jnp.stack([positions // GRID_W, positions % GRID_W], axis=-1).astype(jnp.float32)
    angle = grid[:, :, None] * freqs
    cosine = jnp.cos(angle)[:, None]
    sine = jnp.sin(angle)[:, None]
    parts = matrix.reshape(matrix.shape[:-1] + (2, 2, quarter))
    first = parts[..., 0, :]
    second = parts[..., 1, :]
    turned = jnp.stack([first * cosine - second * sine, second * cosine + first * sine], axis=-2)
    return turned.reshape(matrix.shape)


def on_device(
    queries,
    keys,
    values,
    q_gain,
    k_gain,
    out_weight,
    out_gain,
    residual_in,
    mlp_gain,
    gate_weight,
    up_weight,
    down_weight,
    final_gain,
):
    tok_rows = queries.shape[0]
    head_size = q_gain.shape[0]
    q_heads = queries.shape[1] // head_size
    kv_heads = keys.shape[1] // head_size
    group_size = q_heads // kv_heads
    gate_full, up_full = in_one_piece((gate_weight, up_weight), "sp", 0, 1)
    down_full = lax.all_gather(down_weight, "sp", axis=1, tiled=True)
    positions = lax.axis_index("sp") * tok_rows + jnp.arange(tok_rows, dtype=jnp.int32)
    query_rot = rotary(
        rms_scale(queries.reshape(tok_rows, q_heads, head_size).astype(jnp.float32)) * q_gain,
        positions,
    ).astype(jnp.bfloat16)
    key_rot = rotary(
        rms_scale(keys.reshape(tok_rows, kv_heads, head_size).astype(jnp.float32)) * k_gain,
        positions,
    ).astype(jnp.bfloat16)
    key_flat = key_rot.reshape(tok_rows, kv_heads * head_size)
    grouped = query_rot.reshape(tok_rows, kv_heads, group_size, head_size)
    score_scale = head_size ** (-0.5)
    key_all, value_all = in_one_piece((key_flat, values), "sp", 0, 1)
    total_rows = key_all.shape[0]
    span = math.gcd(total_rows, 1024)
    key_blocks = key_all.reshape(total_rows // span, span, kv_heads, head_size)
    value_blocks = value_all.reshape(total_rows // span, span, kv_heads, head_size)

    def step(run_state, blocks):
        highest, weight_sum, accum = run_state
        key_block, value_block = blocks
        scores = (
            jnp.einsum("qcgd,kcd->cgqk", grouped, key_block, preferred_element_type=jnp.float32)
            * score_scale
        )
        new_high = jnp.maximum(highest, jnp.max(scores, axis=-1))
        factor = jnp.exp(highest - new_high)
        exp_scores = jnp.exp(scores - new_high[..., None])
        weight_sum = weight_sum * factor + jnp.sum(exp_scores, axis=-1)
        accum = accum * factor[..., None] + jnp.einsum(
            "cgqk,kcd->cgqd",
            exp_scores.astype(jnp.bfloat16),
            value_block,
            preferred_element_type=jnp.float32,
        )
        return ((new_high, weight_sum, accum), None)

    start_state = (
        jnp.full((kv_heads, group_size, tok_rows), -1e30, jnp.float32),
        jnp.zeros((kv_heads, group_size, tok_rows), jnp.float32),
        jnp.zeros((kv_heads, group_size, tok_rows, head_size), jnp.float32),
    )
    final_state, unused = lax.scan(step, start_state, (key_blocks, value_blocks))
    highest, weight_sum, accum = final_state
    attended = (
        jnp.transpose(accum / weight_sum[..., None], (2, 0, 1, 3))
        .reshape(tok_rows, q_heads * head_size)
        .astype(jnp.bfloat16)
    )
    head_rows = lax.all_to_all(attended, "tp", split_axis=0, concat_axis=1, tiled=True)
    projected = jnp.dot(head_rows, out_weight, preferred_element_type=jnp.float32)
    mid_stream = (residual_in.astype(jnp.float32) + out_gain * rms_scale(projected)).astype(
        jnp.bfloat16
    )
    normed = (mlp_gain * rms_scale(mid_stream.astype(jnp.float32))).astype(jnp.bfloat16)
    mixer_in = gather_directly(normed, "tp", 0)
    gate_proj = jnp.dot(mixer_in, gate_full, preferred_element_type=jnp.float32)
    up_proj = jnp.dot(mixer_in, up_full, preferred_element_type=jnp.float32)
    hidden = (jax.nn.silu(gate_proj) * up_proj).astype(jnp.bfloat16)
    mlp_branch = sum_at_owner(
        jnp.dot(hidden, down_full, preferred_element_type=jnp.float32).astype(jnp.bfloat16), "tp", 0
    )
    return (mid_stream.astype(jnp.float32) + final_gain * rms_scale(mlp_branch)).astype(
        jnp.bfloat16
    )


def solution(mesh):
    return jax.shard_map(
        on_device,
        mesh=mesh,
        in_specs=(
            P("sp", "tp"),
            P("sp", "tp"),
            P("sp", "tp"),
            P(),
            P(),
            P(),
            P(),
            P(("sp", "tp"), None),
            P(),
            P("sp", "tp"),
            P("sp", "tp"),
            P("tp", "sp"),
            P(),
        ),
        out_specs=P(("sp", "tp"), None),
        check_vma=False,
    )
```

profile of v0, /device:TPU:1, one launch (start us, length us, event | category | flops | bytes accessed | tf_op | source)
XLA Modules:
  0.0 403.7 jit_solution(10065259424443440438)
XLA Ops:
  10.9 1.8 pad_maximum_fusion.1
  15.1 58.4 %all-gather.4.cloned.1.call-done = bf16[16384,256]{0,1:T(8,128)(2,1)} async-done(((bf16[512,256]{0,1:T(8,128)(2,1)}), bf16[16384,256]{0,1:T(8,128)(2,1)}) %all-gather.4.cloned.1.call-update) | async-done | bytes 8388624 | tf_op jit(solution)/shard_map/all_gather | solution.py:17
  73.6 5.8 %fusion.52 = (bf16[16384,128]{0,1:T(8,128)(2,1)}, bf16[16384,128]{0,1:T(8,128)(2,1)}) fusion(bf16[16384,256]{0,1:T(8,128)(2,1)} %all-gather.4.cloned.1.call-done), kind=kLoop, calls=%fused_computation.85 | loop fusion | bytes 16777216 | tf_op jit(solution)/shard_map/split | solution.py:17
  79.4 6.4 %copy.26 = bf16[16384,128]{1,0:T(8,128)(2,1)} copy(bf16[16384,128]{0,1:T(8,128)(2,1)} %get-tuple-element.97) | data formatting | bytes 8388608
  85.8 6.5 %copy.27 = bf16[16384,128]{1,0:T(8,128)(2,1)} copy(bf16[16384,128]{0,1:T(8,128)(2,1)} %get-tuple-element.96) | data formatting | bytes 8388608
  92.3 207.0 %while.15 = (s32[]{:T(128)}, f32[1,4,512]{2,1,0:T(4,128)S(1)}, f32[1,4,512]{2,1,0:T(4,128)S(1)}, f32[1,4,512,128]{3,2,1,0:T(8,128)S(1)}, bf16[16,1024,1,128]{3,1...) while((s32[]{:T(128)}, f32[1,4,512]{2,1,0:T(4,128)S(1)}, ...), condition=%wide.region_5.6_spmd.clone, body=%wide.region_2.5_spmd.clone.sunk | while | flops 1091317760 | bytes 61998208 | solution.py:128
  92.3 5.4 %bitcast_reduce_fusion.3 = (f32[4,512]{1,0:T(4,128)S(1)}, f32[1024,512,4]{1,0,2:T(8,128)}) fusion(bf16[512,1,4,128]{3,0,2,1:T(8,128)(2,1)S(1)} %get-tuple-element.182, bf16[16,1024,1,128]{3,1,2,0:T(8,128)(2,1)} %get-tuple-element.181, s32[]{:T(128)} %get-tuple-element.168), kind=kOutput, calls=%fused_computation.1.clone.1 | convolution fusion | flops 541063168 | bytes 9183744 | tf_op jit(solution)/shard_map/while/body/eval_jaxpr/qcgd,kcd->cgqk/dot_general | solution.py:108
  97.7 4.6 %fusion.67 = f32[1,4,512,128]{3,2,1,0:T(8,128)S(1)} fusion(f32[1024,512,4]{1,0,2:T(8,128)} %get-tuple-element.157, f32[4,512]{1,0:T(4,128)S(1)} %bitcast.101, f32[1,4,512,128]{3,2,1,0:T(8,128)S(1)} %get-tuple-element.171, f32[4,512]{1,0:T(4,128)S(1)} %get-tuple-element.158, pred[]{:T(512)S(6)} %compare.22, ...), kind=kOutput, calls=%fused_computation.10.clone.1 | convolution fusion | flops 543948800 | bytes 10764801 | tf_op jit(solution)/shard_map/while/body/eval_jaxpr/cgqk,kcd->cgqd/dot_general | solution.py:115
  103.6 1.4 fusion.66
  105.1 5.4 %bitcast_reduce_fusion.3 = (f32[4,512]{1,0:T(4,128)S(1)}, f32[1024,512,4]{1,0,2:T(8,128)}) fusion(bf16[512,1,4,128]{3,0,2,1:T(8,128)(2,1)S(1)} %get-tuple-element.182, bf16[16,1024,1,128]{3,1,2,0:T(8,128)(2,1)} %get-tuple-element.181, s32[]{:T(128)} %get-tuple-element.168), kind=kOutput, calls=%fused_computation.1.clone.1 | convolution fusion | flops 541063168 | bytes 9183744 | tf_op jit(solution)/shard_map/while/body/eval_jaxpr/qcgd,kcd->cgqk/dot_general | solution.py:108
  110.5 4.8 %fusion.67 = f32[1,4,512,128]{3,2,1,0:T(8,128)S(1)} fusion(f32[1024,512,4]{1,0,2:T(8,128)} %get-tuple-element.157, f32[4,512]{1,0:T(4,128)S(1)} %bitcast.101, f32[1,4,512,128]{3,2,1,0:T(8,128)S(1)} %get-tuple-element.171, f32[4,512]{1,0:T(4,128)S(1)} %get-tuple-element.158, pred[]{:T(512)S(6)} %compare.22, ...), kind=kOutput, calls=%fused_computation.10.clone.1 | convolution fusion | flops 543948800 | bytes 10764801 | tf_op jit(solution)/shard_map/while/body/eval_jaxpr/cgqk,kcd->cgqd/dot_general | solution.py:115
  115.4 1.5 copy-done
  116.9 1.4 fusion.66
  118.3 5.5 %bitcast_reduce_fusion.3 = (f32[4,512]{1,0:T(4,128)S(1)}, f32[1024,512,4]{1,0,2:T(8,128)}) fusion(bf16[512,1,4,128]{3,0,2,1:T(8,128)(2,1)S(1)} %get-tuple-element.182, bf16[16,1024,1,128]{3,1,2,0:T(8,128)(2,1)} %get-tuple-element.181, s32[]{:T(128)} %get-tuple-element.168), kind=kOutput, calls=%fused_computation.1.clone.1 | convolution fusion | flops 541063168 | bytes 9183744 | tf_op jit(solution)/shard_map/while/body/eval_jaxpr/qcgd,kcd->cgqk/dot_general | solution.py:108
  123.8 5.1 %fusion.67 = f32[1,4,512,128]{3,2,1,0:T(8,128)S(1)} fusion(f32[1024,512,4]{1,0,2:T(8,128)} %get-tuple-element.157, f32[4,512]{1,0:T(4,128)S(1)} %bitcast.101, f32[1,4,512,128]{3,2,1,0:T(8,128)S(1)} %get-tuple-element.171, f32[4,512]{1,0:T(4,128)S(1)} %get-tuple-element.158, pred[]{:T(512)S(6)} %compare.22, ...), kind=kOutput, calls=%fused_computation.10.clone.1 | convolution fusion | flops 543948800 | bytes 10764801 | tf_op jit(solution)/shard_map/while/body/eval_jaxpr/cgqk,kcd->cgqd/dot_general | solution.py:115
  128.9 1.4 copy-done
  130.3 1.4 fusion.66
  131.8 5.5 %bitcast_reduce_fusion.3 = (f32[4,512]{1,0:T(4,128)S(1)}, f32[1024,512,4]{1,0,2:T(8,128)}) fusion(bf16[512,1,4,128]{3,0,2,1:T(8,128)(2,1)S(1)} %get-tuple-element.182, bf16[16,1024,1,128]{3,1,2,0:T(8,128)(2,1)} %get-tuple-element.181, s32[]{:T(128)} %get-tuple-element.168), kind=kOutput, calls=%fused_computation.1.clone.1 | convolution fusion | flops 541063168 | bytes 9183744 | tf_op jit(solution)/shard_map/while/body/eval_jaxpr/qcgd,kcd->cgqk/dot_general | solution.py:108
  137.3 4.6 %fusion.67 = f32[1,4,512,128]{3,2,1,0:T(8,128)S(1)} fusion(f32[1024,512,4]{1,0,2:T(8,128)} %get-tuple-element.157, f32[4,512]{1,0:T(4,128)S(1)} %bitcast.101, f32[1,4,512,128]{3,2,1,0:T(8,128)S(1)} %get-tuple-element.171, f32[4,512]{1,0:T(4,128)S(1)} %get-tuple-element.158, pred[]{:T(512)S(6)} %compare.22, ...), kind=kOutput, calls=%fused_computation.10.clone.1 | convolution fusion | flops 543948800 | bytes 10764801 | tf_op jit(solution)/shard_map/while/body/eval_jaxpr/cgqk,kcd->cgqd/dot_general | solution.py:115
  143.2 1.4 fusion.66
  144.6 5.4 %bitcast_reduce_fusion.3 = (f32[4,512]{1,0:T(4,128)S(1)}, f32[1024,512,4]{1,0,2:T(8,128)}) fusion(bf16[512,1,4,128]{3,0,2,1:T(8,128)(2,1)S(1)} %get-tuple-element.182, bf16[16,1024,1,128]{3,1,2,0:T(8,128)(2,1)} %get-tuple-element.181, s32[]{:T(128)} %get-tuple-element.168), kind=kOutput, calls=%fused_computation.1.clone.1 | convolution fusion | flops 541063168 | bytes 9183744 | tf_op jit(solution)/shard_map/while/body/eval_jaxpr/qcgd,kcd->cgqk/dot_general | solution.py:108
  150.1 4.7 %fusion.67 = f32[1,4,512,128]{3,2,1,0:T(8,128)S(1)} fusion(f32[1024,512,4]{1,0,2:T(8,128)} %get-tuple-element.157, f32[4,512]{1,0:T(4,128)S(1)} %bitcast.101, f32[1,4,512,128]{3,2,1,0:T(8,128)S(1)} %get-tuple-element.171, f32[4,512]{1,0:T(4,128)S(1)} %get-tuple-element.158, pred[]{:T(512)S(6)} %compare.22, ...), kind=kOutput, calls=%fused_computation.10.clone.1 | convolution fusion | flops 543948800 | bytes 10764801 | tf_op jit(solution)/shard_map/while/body/eval_jaxpr/cgqk,kcd->cgqd/dot_general | solution.py:115
  156.1 1.4 fusion.66
  157.5 5.4 %bitcast_reduce_fusion.3 = (f32[4,512]{1,0:T(4,128)S(1)}, f32[1024,512,4]{1,0,2:T(8,128)}) fusion(bf16[512,1,4,128]{3,0,2,1:T(8,128)(2,1)S(1)} %get-tuple-element.182, bf16[16,1024,1,128]{3,1,2,0:T(8,128)(2,1)} %get-tuple-element.181, s32[]{:T(128)} %get-tuple-element.168), kind=kOutput, calls=%fused_computation.1.clone.1 | convolution fusion | flops 541063168 | bytes 9183744 | tf_op jit(solution)/shard_map/while/body/eval_jaxpr/qcgd,kcd->cgqk/dot_general | solution.py:108
  163.0 4.6 %fusion.67 = f32[1,4,512,128]{3,2,1,0:T(8,128)S(1)} fusion(f32[1024,512,4]{1,0,2:T(8,128)} %get-tuple-element.157, f32[4,512]{1,0:T(4,128)S(1)} %bitcast.101, f32[1,4,512,128]{3,2,1,0:T(8,128)S(1)} %get-tuple-element.171, f32[4,512]{1,0:T(4,128)S(1)} %get-tuple-element.158, pred[]{:T(512)S(6)} %compare.22, ...), kind=kOutput, calls=%fused_computation.10.clone.1 | convolution fusion | flops 543948800 | bytes 10764801 | tf_op jit(solution)/shard_map/while/body/eval_jaxpr/cgqk,kcd->cgqd/dot_general | solution.py:115
  167.6 1.8 copy-done
  169.3 1.4 fusion.66
  170.8 5.4 %bitcast_reduce_fusion.3 = (f32[4,512]{1,0:T(4,128)S(1)}, f32[1024,512,4]{1,0,2:T(8,128)}) fusion(bf16[512,1,4,128]{3,0,2,1:T(8,128)(2,1)S(1)} %get-tuple-element.182, bf16[16,1024,1,128]{3,1,2,0:T(8,128)(2,1)} %get-tuple-element.181, s32[]{:T(128)} %get-tuple-element.168), kind=kOutput, calls=%fused_computation.1.clone.1 | convolution fusion | flops 541063168 | bytes 9183744 | tf_op jit(solution)/shard_map/while/body/eval_jaxpr/qcgd,kcd->cgqk/dot_general | solution.py:108
  176.2 4.9 %fusion.67 = f32[1,4,512,128]{3,2,1,0:T(8,128)S(1)} fusion(f32[1024,512,4]{1,0,2:T(8,128)} %get-tuple-element.157, f32[4,512]{1,0:T(4,128)S(1)} %bitcast.101, f32[1,4,512,128]{3,2,1,0:T(8,128)S(1)} %get-tuple-element.171, f32[4,512]{1,0:T(4,128)S(1)} %get-tuple-element.158, pred[]{:T(512)S(6)} %compare.22, ...), kind=kOutput, calls=%fused_computation.10.clone.1 | convolution fusion | flops 543948800 | bytes 10764801 | tf_op jit(solution)/shard_map/while/body/eval_jaxpr/cgqk,kcd->cgqd/dot_general | solution.py:115
  181.1 1.6 copy-done
  182.7 1.4 fusion.66
  184.1 5.4 %bitcast_reduce_fusion.3 = (f32[4,512]{1,0:T(4,128)S(1)}, f32[1024,512,4]{1,0,2:T(8,128)}) fusion(bf16[512,1,4,128]{3,0,2,1:T(8,128)(2,1)S(1)} %get-tuple-element.182, bf16[16,1024,1,128]{3,1,2,0:T(8,128)(2,1)} %get-tuple-element.181, s32[]{:T(128)} %get-tuple-element.168), kind=kOutput, calls=%fused_computation.1.clone.1 | convolution fusion | flops 541063168 | bytes 9183744 | tf_op jit(solution)/shard_map/while/body/eval_jaxpr/qcgd,kcd->cgqk/dot_general | solution.py:108
  189.6 4.6 %fusion.67 = f32[1,4,512,128]{3,2,1,0:T(8,128)S(1)} fusion(f32[1024,512,4]{1,0,2:T(8,128)} %get-tuple-element.157, f32[4,512]{1,0:T(4,128)S(1)} %bitcast.101, f32[1,4,512,128]{3,2,1,0:T(8,128)S(1)} %get-tuple-element.171, f32[4,512]{1,0:T(4,128)S(1)} %get-tuple-element.158, pred[]{:T(512)S(6)} %compare.22, ...), kind=kOutput, calls=%fused_computation.10.clone.1 | convolution fusion | flops 543948800 | bytes 10764801 | tf_op jit(solution)/shard_map/while/body/eval_jaxpr/cgqk,kcd->cgqd/dot_general | solution.py:115
  195.5 1.4 fusion.66
  196.9 5.4 %bitcast_reduce_fusion.3 = (f32[4,512]{1,0:T(4,128)S(1)}, f32[1024,512,4]{1,0,2:T(8,128)}) fusion(bf16[512,1,4,128]{3,0,2,1:T(8,128)(2,1)S(1)} %get-tuple-element.182, bf16[16,1024,1,128]{3,1,2,0:T(8,128)(2,1)} %get-tuple-element.181, s32[]{:T(128)} %get-tuple-element.168), kind=kOutput, calls=%fused_computation.1.clone.1 | convolution fusion | flops 541063168 | bytes 9183744 | tf_op jit(solution)/shard_map/while/body/eval_jaxpr/qcgd,kcd->cgqk/dot_general | solution.py:108
  202.4 4.6 %fusion.67 = f32[1,4,512,128]{3,2,1,0:T(8,128)S(1)} fusion(f32[1024,512,4]{1,0,2:T(8,128)} %get-tuple-element.157, f32[4,512]{1,0:T(4,128)S(1)} %bitcast.101, f32[1,4,512,128]{3,2,1,0:T(8,128)S(1)} %get-tuple-element.171, f32[4,512]{1,0:T(4,128)S(1)} %get-tuple-element.158, pred[]{:T(512)S(6)} %compare.22, ...), kind=kOutput, calls=%fused_computation.10.clone.1 | convolution fusion | flops 543948800 | bytes 10764801 | tf_op jit(solution)/shard_map/while/body/eval_jaxpr/cgqk,kcd->cgqd/dot_general | solution.py:115
  208.3 1.4 fusion.66
  209.7 5.4 %bitcast_reduce_fusion.3 = (f32[4,512]{1,0:T(4,128)S(1)}, f32[1024,512,4]{1,0,2:T(8,128)}) fusion(bf16[512,1,4,128]{3,0,2,1:T(8,128)(2,1)S(1)} %get-tuple-element.182, bf16[16,1024,1,128]{3,1,2,0:T(8,128)(2,1)} %get-tuple-element.181, s32[]{:T(128)} %get-tuple-element.168), kind=kOutput, calls=%fused_computation.1.clone.1 | convolution fusion | flops 541063168 | bytes 9183744 | tf_op jit(solution)/shard_map/while/body/eval_jaxpr/qcgd,kcd->cgqk/dot_general | solution.py:108
  215.2 4.6 %fusion.67 = f32[1,4,512,128]{3,2,1,0:T(8,128)S(1)} fusion(f32[1024,512,4]{1,0,2:T(8,128)} %get-tuple-element.157, f32[4,512]{1,0:T(4,128)S(1)} %bitcast.101, f32[1,4,512,128]{3,2,1,0:T(8,128)S(1)} %get-tuple-element.171, f32[4,512]{1,0:T(4,128)S(1)} %get-tuple-element.158, pred[]{:T(512)S(6)} %compare.22, ...), kind=kOutput, calls=%fused_computation.10.clone.1 | convolution fusion | flops 543948800 | bytes 10764801 | tf_op jit(solution)/shard_map/while/body/eval_jaxpr/cgqk,kcd->cgqd/dot_general | solution.py:115
  221.1 1.4 fusion.66
  222.5 5.4 %bitcast_reduce_fusion.3 = (f32[4,512]{1,0:T(4,128)S(1)}, f32[1024,512,4]{1,0,2:T(8,128)}) fusion(bf16[512,1,4,128]{3,0,2,1:T(8,128)(2,1)S(1)} %get-tuple-element.182, bf16[16,1024,1,128]{3,1,2,0:T(8,128)(2,1)} %get-tuple-element.181, s32[]{:T(128)} %get-tuple-element.168), kind=kOutput, calls=%fused_computation.1.clone.1 | convolution fusion | flops 541063168 | bytes 9183744 | tf_op jit(solution)/shard_map/while/body/eval_jaxpr/qcgd,kcd->cgqk/dot_general | solution.py:108
  228.0 4.6 %fusion.67 = f32[1,4,512,128]{3,2,1,0:T(8,128)S(1)} fusion(f32[1024,512,4]{1,0,2:T(8,128)} %get-tuple-element.157, f32[4,512]{1,0:T(4,128)S(1)} %bitcast.101, f32[1,4,512,128]{3,2,1,0:T(8,128)S(1)} %get-tuple-element.171, f32[4,512]{1,0:T(4,128)S(1)} %get-tuple-element.158, pred[]{:T(512)S(6)} %compare.22, ...), kind=kOutput, calls=%fused_computation.10.clone.1 | convolution fusion | flops 543948800 | bytes 10764801 | tf_op jit(solution)/shard_map/while/body/eval_jaxpr/cgqk,kcd->cgqd/dot_general | solution.py:115
  233.9 1.4 fusion.66
  235.3 5.4 %bitcast_reduce_fusion.3 = (f32[4,512]{1,0:T(4,128)S(1)}, f32[1024,512,4]{1,0,2:T(8,128)}) fusion(bf16[512,1,4,128]{3,0,2,1:T(8,128)(2,1)S(1)} %get-tuple-element.182, bf16[16,1024,1,128]{3,1,2,0:T(8,128)(2,1)} %get-tuple-element.181, s32[]{:T(128)} %get-tuple-element.168), kind=kOutput, calls=%fused_computation.1.clone.1 | convolution fusion | flops 541063168 | bytes 9183744 | tf_op jit(solution)/shard_map/while/body/eval_jaxpr/qcgd,kcd->cgqk/dot_general | solution.py:108
  240.8 4.6 %fusion.67 = f32[1,4,512,128]{3,2,1,0:T(8,128)S(1)} fusion(f32[1024,512,4]{1,0,2:T(8,128)} %get-tuple-element.157, f32[4,512]{1,0:T(4,128)S(1)} %bitcast.101, f32[1,4,512,128]{3,2,1,0:T(8,128)S(1)} %get-tuple-element.171, f32[4,512]{1,0:T(4,128)S(1)} %get-tuple-element.158, pred[]{:T(512)S(6)} %compare.22, ...), kind=kOutput, calls=%fused_computation.10.clone.1 | convolution fusion | flops 543948800 | bytes 10764801 | tf_op jit(solution)/shard_map/while/body/eval_jaxpr/cgqk,kcd->cgqd/dot_general | solution.py:115
  246.7 1.4 fusion.66
  248.1 5.4 %bitcast_reduce_fusion.3 = (f32[4,512]{1,0:T(4,128)S(1)}, f32[1024,512,4]{1,0,2:T(8,128)}) fusion(bf16[512,1,4,128]{3,0,2,1:T(8,128)(2,1)S(1)} %get-tuple-element.182, bf16[16,1024,1,128]{3,1,2,0:T(8,128)(2,1)} %get-tuple-element.181, s32[]{:T(128)} %get-tuple-element.168), kind=kOutput, calls=%fused_computation.1.clone.1 | convolution fusion | flops 541063168 | bytes 9183744 | tf_op jit(solution)/shard_map/while/body/eval_jaxpr/qcgd,kcd->cgqk/dot_general | solution.py:108
  253.5 4.6 %fusion.67 = f32[1,4,512,128]{3,2,1,0:T(8,128)S(1)} fusion(f32[1024,512,4]{1,0,2:T(8,128)} %get-tuple-element.157, f32[4,512]{1,0:T(4,128)S(1)} %bitcast.101, f32[1,4,512,128]{3,2,1,0:T(8,128)S(1)} %get-tuple-element.171, f32[4,512]{1,0:T(4,128)S(1)} %get-tuple-element.158, pred[]{:T(512)S(6)} %compare.22, ...), kind=kOutput, calls=%fused_computation.10.clone.1 | convolution fusion | flops 543948800 | bytes 10764801 | tf_op jit(solution)/shard_map/while/body/eval_jaxpr/cgqk,kcd->cgqd/dot_general | solution.py:115
  259.4 1.4 fusion.66
  260.9 5.4 %bitcast_reduce_fusion.3 = (f32[4,512]{1,0:T(4,128)S(1)}, f32[1024,512,4]{1,0,2:T(8,128)}) fusion(bf16[512,1,4,128]{3,0,2,1:T(8,128)(2,1)S(1)} %get-tuple-element.182, bf16[16,1024,1,128]{3,1,2,0:T(8,128)(2,1)} %get-tuple-element.181, s32[]{:T(128)} %get-tuple-element.168), kind=kOutput, calls=%fused_computation.1.clone.1 | convolution fusion | flops 541063168 | bytes 9183744 | tf_op jit(solution)/shard_map/while/body/eval_jaxpr/qcgd,kcd->cgqk/dot_general | solution.py:108
  266.3 4.6 %fusion.67 = f32[1,4,512,128]{3,2,1,0:T(8,128)S(1)} fusion(f32[1024,512,4]{1,0,2:T(8,128)} %get-tuple-element.157, f32[4,512]{1,0:T(4,128)S(1)} %bitcast.101, f32[1,4,512,128]{3,2,1,0:T(8,128)S(1)} %get-tuple-element.171, f32[4,512]{1,0:T(4,128)S(1)} %get-tuple-element.158, pred[]{:T(512)S(6)} %compare.22, ...), kind=kOutput, calls=%fused_computation.10.clone.1 | convolution fusion | flops 543948800 | bytes 10764801 | tf_op jit(solution)/shard_map/while/body/eval_jaxpr/cgqk,kcd->cgqd/dot_general | solution.py:115
  272.2 1.4 fusion.66
  273.7 5.4 %bitcast_reduce_fusion.3 = (f32[4,512]{1,0:T(4,128)S(1)}, f32[1024,512,4]{1,0,2:T(8,128)}) fusion(bf16[512,1,4,128]{3,0,2,1:T(8,128)(2,1)S(1)} %get-tuple-element.182, bf16[16,1024,1,128]{3,1,2,0:T(8,128)(2,1)} %get-tuple-element.181, s32[]{:T(128)} %get-tuple-element.168), kind=kOutput, calls=%fused_computation.1.clone.1 | convolution fusion | flops 541063168 | bytes 9183744 | tf_op jit(solution)/shard_map/while/body/eval_jaxpr/qcgd,kcd->cgqk/dot_general | solution.py:108
  279.1 4.6 %fusion.67 = f32[1,4,512,128]{3,2,1,0:T(8,128)S(1)} fusion(f32[1024,512,4]{1,0,2:T(8,128)} %get-tuple-element.157, f32[4,512]{1,0:T(4,128)S(1)} %bitcast.101, f32[1,4,512,128]{3,2,1,0:T(8,128)S(1)} %get-tuple-element.171, f32[4,512]{1,0:T(4,128)S(1)} %get-tuple-element.158, pred[]{:T(512)S(6)} %compare.22, ...), kind=kOutput, calls=%fused_computation.10.clone.1 | convolution fusion | flops 543948800 | bytes 10764801 | tf_op jit(solution)/shard_map/while/body/eval_jaxpr/cgqk,kcd->cgqd/dot_general | solution.py:115
  285.0 1.4 fusion.66
  286.5 5.4 %bitcast_reduce_fusion.3 = (f32[4,512]{1,0:T(4,128)S(1)}, f32[1024,512,4]{1,0,2:T(8,128)}) fusion(bf16[512,1,4,128]{3,0,2,1:T(8,128)(2,1)S(1)} %get-tuple-element.182, bf16[16,1024,1,128]{3,1,2,0:T(8,128)(2,1)} %get-tuple-element.181, s32[]{:T(128)} %get-tuple-element.168), kind=kOutput, calls=%fused_computation.1.clone.1 | convolution fusion | flops 541063168 | bytes 9183744 | tf_op jit(solution)/shard_map/while/body/eval_jaxpr/qcgd,kcd->cgqk/dot_general | solution.py:108
  291.9 4.6 %fusion.67 = f32[1,4,512,128]{3,2,1,0:T(8,128)S(1)} fusion(f32[1024,512,4]{1,0,2:T(8,128)} %get-tuple-element.157, f32[4,512]{1,0:T(4,128)S(1)} %bitcast.101, f32[1,4,512,128]{3,2,1,0:T(8,128)S(1)} %get-tuple-element.171, f32[4,512]{1,0:T(4,128)S(1)} %get-tuple-element.158, pred[]{:T(512)S(6)} %compare.22, ...), kind=kOutput, calls=%fused_computation.10.clone.1 | convolution fusion | flops 543948800 | bytes 10764801 | tf_op jit(solution)/shard_map/while/body/eval_jaxpr/cgqk,kcd->cgqd/dot_general | solution.py:115
  297.8 1.4 fusion.66
  300.2 13.0 %all_to_all.26 = bf16[4,128,512]{2,1,0:T(8,128)(2,1)S(1)} all-to-all(bf16[4,128,512]{2,1,0:T(8,128)(2,1)S(1)} %convert_element_type.88), channel_id=1, replica_groups=mesh['sp'=32,'tp'=4] {'tp'}, dimensions={0} | all-to-all | bytes 1048576 | tf_op jit(solution)/shard_map/all_to_all | solution.py:135
  313.5 4.8 %multiply_reduce_fusion.1 = (f32[128]{0:T(128)S(1)}, f32[128,2048]{1,0:T(8,128)S(1)}) fusion(bf16[128,2048]{0,1:T(8,128)(2,1)S(1)} %bitcast.104, bf16[2048,2048]{1,0:T(8,128)(2,1)} %param.20), kind=kOutput, calls=%fused_computation.44 | convolution fusion | flops 1074265984 | bytes 9961984 | tf_op jit(solution)/shard_map/dot_general | solution.py:136
  319.2 27.7 %all_to_all.27 = bf16[4,128,2048]{2,1,0:T(8,128)(2,1)S(1)} all-to-all(bf16[4,128,2048]{2,1,0:T(8,128)(2,1)S(1)} %broadcast_in_dim.11), channel_id=1, replica_groups=mesh['sp'=32,'tp'=4] {'tp'}, dimensions={0} | all-to-all | bytes 4194304 | tf_op jit(solution)/shard_map/all_to_all | solution.py:28
  346.9 7.6 %fusion.26 = f32[512,1408]{1,0:T(8,128)} fusion(bf16[512,2048]{1,0:T(8,128)(2,1)S(1)} %bitcast.105, bf16[2048,2816]{1,0:T(8,128)(2,1)} %all-gather.6.cloned.1.call-done), kind=kOutput, calls=%fused_computation.28 | convolution fusion | flops 2952790016 | bytes 10747904 | tf_op jit(solution)/shard_map/dot_general | solution.py:142
  354.5 13.2 %convolution_convert_fusion = bf16[512,2048]{1,0:T(8,128)(2,1)} fusion(bf16[1408,2048]{0,1:T(8,128)(2,1)} %all-gather.8.cloned.1.call-done, bf16[512,2048]{1,0:T(8,128)(2,1)S(1)} %bitcast.106, bf16[2048,2816]{1,0:T(8,128)(2,1)} %all-gather.6.cloned.1.call-done, f32[512,1408]{1,0:T(8,128)} %fusion.26), kind=kOutput, calls=%fused_computation.33 | convolution fusion | flops 5910953984 | bytes 18612224 | tf_op jit(solution)/shard_map/dot_general | solution.py:146
  367.8 27.8 %all_to_all.28 = bf16[4,128,2048]{2,1,0:T(8,128)(2,1)S(1)} all-to-all(bf16[4,128,2048]{2,1,0:T(8,128)(2,1)} %bitcast.107), channel_id=1, replica_groups=mesh['sp'=32,'tp'=4] {'tp'}, dimensions={0} | all-to-all | bytes 4194304 | tf_op jit(solution)/shard_map/all_to_all | solution.py:42
  (132 shorter events, 26.5 us)
Async XLA Ops:
  6.5 7.5 %copy-start.1 = (bf16[512,512]{1,0:T(8,128)(2,1)S(1)}, bf16[512,512]{1,0:T(8,128)(2,1)}, u32[]{:S(2)}) copy-start(bf16[512,512]{1,0:T(8,128)(2,1)} %param.15) | copy-start | bytes 1572868
  6.5 7.8 %copy-start.6 = (f32[128]{0:T(128)S(1)}, f32[128]{0:T(128)}, u32[]{:S(2)}) copy-start(f32[128]{0:T(128)} %param.18) | copy-start | bytes 1540
  6.5 67.0 %all-gather.4.cloned.1.call-start = ((), (), s32[]{:S(2)}) async-start(), calls=%async_computation.3 | async-start | bytes 8650752 | tf_op jit(solution)/shard_map/all_gather | solution.py:17
  10.8 336.1 %all-gather.6.cloned.1.call-start = ((), (), s32[]{:S(2)}) async-start(), calls=%async_computation.4 | async-start | bytes 11894784 | tf_op jit(solution)/shard_map/all_gather | solution.py:17
  12.7 341.8 %all-gather.8.cloned.1.call-start = ((), (), s32[]{:S(2)}) async-start(), calls=%async_computation.5 | async-start | bytes 5947392 | tf_op jit(solution)/shard_map/all_gather | solution.py:85
  97.7 5.9 %copy-start = (f32[1024,512,4]{1,0,2:T(8,128)S(1)}, f32[1024,512,4]{1,0,2:T(8,128)}, u32[]{:S(2)}) copy-start(f32[1024,512,4]{1,0,2:T(8,128)} %get-tuple-element.157) | copy-start | bytes 25165828 | tf_op jit(solution)/shard_map/while
  110.5 6.4 %copy-start = (f32[1024,512,4]{1,0,2:T(8,128)S(1)}, f32[1024,512,4]{1,0,2:T(8,128)}, u32[]{:S(2)}) copy-start(f32[1024,512,4]{1,0,2:T(8,128)} %get-tuple-element.157) | copy-start | bytes 25165828 | tf_op jit(solution)/shard_map/while
  123.8 6.5 %copy-start = (f32[1024,512,4]{1,0,2:T(8,128)S(1)}, f32[1024,512,4]{1,0,2:T(8,128)}, u32[]{:S(2)}) copy-start(f32[1024,512,4]{1,0,2:T(8,128)} %get-tuple-element.157) | copy-start | bytes 25165828 | tf_op jit(solution)/shard_map/while
  137.3 5.9 %copy-start = (f32[1024,512,4]{1,0,2:T(8,128)S(1)}, f32[1024,512,4]{1,0,2:T(8,128)}, u32[]{:S(2)}) copy-start(f32[1024,512,4]{1,0,2:T(8,128)} %get-tuple-element.157) | copy-start | bytes 25165828 | tf_op jit(solution)/shard_map/while
  150.1 6.0 %copy-start = (f32[1024,512,4]{1,0,2:T(8,128)S(1)}, f32[1024,512,4]{1,0,2:T(8,128)}, u32[]{:S(2)}) copy-start(f32[1024,512,4]{1,0,2:T(8,128)} %get-tuple-element.157) | copy-start | bytes 25165828 | tf_op jit(solution)/shard_map/while
  162.9 6.4 %copy-start = (f32[1024,512,4]{1,0,2:T(8,128)S(1)}, f32[1024,512,4]{1,0,2:T(8,128)}, u32[]{:S(2)}) copy-start(f32[1024,512,4]{1,0,2:T(8,128)} %get-tuple-element.157) | copy-start | bytes 25165828 | tf_op jit(solution)/shard_map/while
  176.2 6.5 %copy-start = (f32[1024,512,4]{1,0,2:T(8,128)S(1)}, f32[1024,512,4]{1,0,2:T(8,128)}, u32[]{:S(2)}) copy-start(f32[1024,512,4]{1,0,2:T(8,128)} %get-tuple-element.157) | copy-start | bytes 25165828 | tf_op jit(solution)/shard_map/while
  189.6 5.9 %copy-start = (f32[1024,512,4]{1,0,2:T(8,128)S(1)}, f32[1024,512,4]{1,0,2:T(8,128)}, u32[]{:S(2)}) copy-start(f32[1024,512,4]{1,0,2:T(8,128)} %get-tuple-element.157) | copy-start | bytes 25165828 | tf_op jit(solution)/shard_map/while
  202.4 5.9 %copy-start = (f32[1024,512,4]{1,0,2:T(8,128)S(1)}, f32[1024,512,4]{1,0,2:T(8,128)}, u32[]{:S(2)}) copy-start(f32[1024,512,4]{1,0,2:T(8,128)} %get-tuple-element.157) | copy-start | bytes 25165828 | tf_op jit(solution)/shard_map/while
  215.2 5.9 %copy-start = (f32[1024,512,4]{1,0,2:T(8,128)S(1)}, f32[1024,512,4]{1,0,2:T(8,128)}, u32[]{:S(2)}) copy-start(f32[1024,512,4]{1,0,2:T(8,128)} %get-tuple-element.157) | copy-start | bytes 25165828 | tf_op jit(solution)/shard_map/while
  227.9 5.9 %copy-start = (f32[1024,512,4]{1,0,2:T(8,128)S(1)}, f32[1024,512,4]{1,0,2:T(8,128)}, u32[]{:S(2)}) copy-start(f32[1024,512,4]{1,0,2:T(8,128)} %get-tuple-element.157) | copy-start | bytes 25165828 | tf_op jit(solution)/shard_map/while
  240.7 5.9 %copy-start = (f32[1024,512,4]{1,0,2:T(8,128)S(1)}, f32[1024,512,4]{1,0,2:T(8,128)}, u32[]{:S(2)}) copy-start(f32[1024,512,4]{1,0,2:T(8,128)} %get-tuple-element.157) | copy-start | bytes 25165828 | tf_op jit(solution)/shard_map/while
  253.5 5.9 %copy-start = (f32[1024,512,4]{1,0,2:T(8,128)S(1)}, f32[1024,512,4]{1,0,2:T(8,128)}, u32[]{:S(2)}) copy-start(f32[1024,512,4]{1,0,2:T(8,128)} %get-tuple-element.157) | copy-start | bytes 25165828 | tf_op jit(solution)/shard_map/while
  266.3 5.9 %copy-start = (f32[1024,512,4]{1,0,2:T(8,128)S(1)}, f32[1024,512,4]{1,0,2:T(8,128)}, u32[]{:S(2)}) copy-start(f32[1024,512,4]{1,0,2:T(8,128)} %get-tuple-element.157) | copy-start | bytes 25165828 | tf_op jit(solution)/shard_map/while
  279.1 5.9 %copy-start = (f32[1024,512,4]{1,0,2:T(8,128)S(1)}, f32[1024,512,4]{1,0,2:T(8,128)}, u32[]{:S(2)}) copy-start(f32[1024,512,4]{1,0,2:T(8,128)} %get-tuple-element.157) | copy-start | bytes 25165828 | tf_op jit(solution)/shard_map/while
  291.9 5.9 %copy-start = (f32[1024,512,4]{1,0,2:T(8,128)S(1)}, f32[1024,512,4]{1,0,2:T(8,128)}, u32[]{:S(2)}) copy-start(f32[1024,512,4]{1,0,2:T(8,128)} %get-tuple-element.157) | copy-start | bytes 25165828 | tf_op jit(solution)/shard_map/while
  313.5 4.8 %copy-start.2 = (bf16[128,2048]{1,0:T(8,128)(2,1)S(1)}, bf16[128,2048]{1,0:T(8,128)(2,1)}, u32[]{:S(2)}) copy-start(bf16[128,2048]{1,0:T(8,128)(2,1)} %param.22) | copy-start | bytes 1572868
  313.5 4.8 %copy-start.3 = (f32[2048]{0:T(1024)S(1)}, f32[2048]{0:T(1024)}, u32[]{:S(2)}) copy-start(f32[2048]{0:T(1024)} %param.21) | copy-start | bytes 24580
  313.5 5.2 %copy-start.4 = (f32[2048]{0:T(1024)S(1)}, f32[2048]{0:T(1024)}, u32[]{:S(2)}) copy-start(f32[2048]{0:T(1024)} %param.23) | copy-start | bytes 24580
  367.8 28.3 %copy-start.5 = (f32[2048]{0:T(1024)S(1)}, f32[2048]{0:T(1024)}, u32[]{:S(2)}) copy-start(f32[2048]{0:T(1024)} %param.27) | copy-start | bytes 24580
Sparse Core Ops, SparseCore 0:
  11.0 62.5 all-gather.3
  75.8 59.9 all-gather.5
  138.0 47.6 all-gather.7
where the time goes:
time: 407 us; the launch traced here: 404 us
  matrix products  187 us (46%)
  blocking collectives  68.5 us (17%)
  waiting for transfers between devices  59.1 us (15%)
  local copies, waits for them, and re-layouts  44.5 us (11%)
  other arithmetic  30 us (7%)
  between operations  13.4 us (3%)
    dot_general x16, matrix products, step(): jnp.einsum('qcgd,kcd->cgqk', grouped, key_block, preferred_element_type=j...  87.1 us
    dot_general x16, matrix products, step(): jnp.einsum('cgqk,kcd->cgqd', exp_scores.astype(jnp.bfloat16), value_block...  74.6 us
    all_gather x2, waiting for transfers between devices, in_one_piece(): lax.all_gather(both, axis, axis=dim, tiled=True)  58.4 us
    all_to_all x1, blocking collectives, sum_at_owner(): lax.all_to_all(pieces, axis, split_axis=0, concat_axis=0, tiled=True)  27.8 us
    all_to_all x1, blocking collectives, copy_for_each(): return lax.all_to_all(copies, axis, split_axis=0, concat_axis=0, tiled=True)  27.7 us
    reduce_sum x16, other arithmetic, step(): weight_sum = weight_sum * factor + jnp.sum(exp_scores, axis=-1)  22 us
    while x48, local copies, waits for them, and re-layouts  22 us
    unnamed x18, local copies, waits for them, and re-layouts  15.4 us
  transfers between devices with their start and end apart: 3, of which 1 were waited for; matrix products, arithmetic and copies ran while one was open for 55% of the time, Pallas kernels for 0%

commit v1 on v0

v1 whole, which is shorter than its diff:
```python
import functools
import math

import jax
import jax.numpy as jnp
from jax import lax
from jax.experimental import pallas as pl
from jax.experimental.pallas import tpu as pltpu
from jax.sharding import PartitionSpec as P

GRID_W = 64
MESH = pl.DeviceIdType.MESH
EPS = 1e-06
LOG2_SCALE = 128 ** (-0.5) * math.log2(math.e)
UNIT = 512
PHASE1 = 10

RING = [
    ("A", 1, (0, 0), None, (-1, 0)),
    ("A", -1, (0, 0), None, (1, 0)),
    ("B", 1, (0, 0), None, (0, -1)),
    ("B", -1, (0, 0), None, (0, 1)),
    ("A", 1, (-1, 0), 0, (2, 0)),
    ("A", -1, (1, 0), 1, (2, 0)),
    ("B", 1, (-1, 0), None, (-1, -1)),
    ("B", -1, (-1, 0), None, (-1, 1)),
    ("B", 1, (1, 0), None, (1, -1)),
    ("B", -1, (1, 0), None, (1, 1)),
    ("B", 1, (0, -1), 0, (0, 2)),
    ("B", -1, (0, 1), 1, (0, 2)),
    ("B", 1, (2, 0), None, (2, -1)),
    ("B", -1, (2, 0), None, (2, 1)),
    ("B", 1, (-1, -1), 0, (-1, 2)),
    ("B", -1, (-1, 1), 1, (-1, 2)),
    ("B", 1, (1, -1), 0, (1, 2)),
    ("B", -1, (1, 1), 1, (1, 2)),
    ("B", 1, (2, -1), 0, (2, 2)),
    ("B", -1, (2, 1), 1, (2, 2)),
]
PLACES = [(0, 0), (-1, 0), (1, 0), (0, -1), (0, 1), (2, 0), (0, 2), (-1, -1), (-1, 1), (1, -1), (1, 1), (2, -1), (2, 1), (-1, 2), (1, 2), (2, 2)]
STAGES = [
    ([], [0, 1, 2, 3], [(0, 0)]),
    ([0, 1, 2, 3], [4, 5, 10, 11, 6, 7, 8, 9], [(-1, 0), (1, 0), (0, -1), (0, 1)]),
    ([4, 5, 10, 11, 6, 7, 8, 9], [12, 13, 14, 15, 16, 17], [(2, 0), (0, 2), (-1, -1), (-1, 1), (1, -1), (1, 1)]),
    ([12, 13, 14, 15, 16, 17], [18, 19], [(2, -1), (2, 1), (-1, 2), (1, 2)]),
    ([18, 19], [], [(2, 2)]),
]
OWN_SLOT = {(0, 0): 0, (-1, 0): 2, (1, 0): 3, (0, -1): 4, (0, 1): 5, (2, 0): 10, (0, 2): 11, (-1, -1): 12, (-1, 1): 13, (1, -1): 14, (1, 1): 15,
            (2, -1): 22, (2, 1): 23, (-1, 2): 24, (1, 2): 25, (2, 2): 30}
PARTNER_SLOT = {(0, 0): 1, (-1, 0): 6, (1, 0): 7, (0, -1): 8, (0, 1): 9, (2, 0): 16, (0, 2): 17, (-1, -1): 18, (-1, 1): 19, (1, -1): 20, (1, 1): 21,
                (2, -1): 26, (2, 1): 27, (-1, 2): 28, (1, 2): 29, (2, 2): 31}
N_COPIES = len(RING) + len(PLACES)


def normalized(x):
    return x * lax.rsqrt(jnp.mean(x * x, axis=-1, keepdims=True) + EPS)


def layer_kernel(n, tp, q_ref, k_ref, v_ref, cos_ref, sin_ref, qg_ref, kg_ref, og_ref, mg_ref, fg_ref,
                 ow_hbm, res_hbm, gate_hbm, up_hbm, down_hbm, out_ref,
                 kv, gu, dt, ow, res, att, mid, nrm, hid, part, recv, proj, qt, s0, s1, acc, m_ref, l_ref,
                 send_sem, recv_sem, x_send, x_recv, local_sem):
    a = lax.axis_index("sp")
    t = lax.axis_index("tp")
    c = lax.rem(a, 2)
    chip = lax.div(a, 2)
    z = lax.div(chip, n)
    y = lax.rem(chip, n)
    u = y * (1 - c) + z * c
    w = z * (1 - c) + y * c
    partner = a + 1 - 2 * c

    def device_at(uu, ww, cc):
        return ((ww * (1 - cc) + uu * cc) * n + uu * (1 - cc) + ww * cc) * 2 + cc

    def own_index(du, dw):
        return device_at(lax.rem(u + du + n, n), lax.rem(w + dw + n, n), c)

    def partner_index(du, dw):
        return device_at(lax.rem(w + du + n, n), lax.rem(u + dw + n, n), 1 - c)

    neighbour = {("A", 1): own_index(1, 0), ("A", -1): own_index(-1, 0), ("B", 1): own_index(0, 1), ("B", -1): own_index(0, -1)}
    peers = [lax.rem(t + d, tp) for d in range(1, tp)]

    class Gather:
        def __init__(self, number, buffer, by_slot):
            self.base, self.buffer, self.by_slot = number * N_COPIES, buffer, by_slot
            self.half_rows = buffer.shape[1] // 2

        def view(self, index, half):
            if half is None:
                return self.buffer.at[index]
            return self.buffer.at[index, pl.ds(half * self.half_rows, self.half_rows)]

        def own(self, place):
            return OWN_SLOT[place] if self.by_slot else own_index(*place)

        def ring(self, i):
            axis, sign, source, half, landing = RING[i]
            at = self.own(source)
            to = OWN_SLOT[landing] if self.by_slot else at
            return pltpu.make_async_remote_copy(
                src_ref=self.view(at, half), dst_ref=self.view(to, half),
                send_sem=send_sem.at[self.base + i], recv_sem=recv_sem.at[self.base + i],
                device_id=(neighbour[axis, sign], t), device_id_type=MESH)

        def ring_arrival(self, i):
            half, landing = RING[i][3:]
            here = self.view(self.own(landing), half)
            return pltpu.make_async_remote_copy(
                src_ref=here, dst_ref=here,
                send_sem=send_sem.at[self.base + i], recv_sem=recv_sem.at[self.base + i],
                device_id=(partner, t), device_id_type=MESH)

        def push(self, place):
            i = self.base + len(RING) + PLACES.index(place)
            at = self.own(place)
            to = PARTNER_SLOT[place] if self.by_slot else at
            return pltpu.make_async_remote_copy(
                src_ref=self.view(at, None), dst_ref=self.view(to, None),
                send_sem=send_sem.at[i], recv_sem=recv_sem.at[i],
                device_id=(partner, t), device_id_type=MESH)

        def push_arrival(self, place):
            i = self.base + len(RING) + PLACES.index(place)
            here = self.view(PARTNER_SLOT[place] if self.by_slot else partner_index(*place), None)
            return pltpu.make_async_remote_copy(
                src_ref=here, dst_ref=here, send_sem=send_sem.at[i], recv_sem=recv_sem.at[i],
                device_id=(partner, t), device_id_type=MESH)

        def stage(self, number):
            waits, sends, pushes = STAGES[number - 1]
            for i in waits:
                self.ring_arrival(i).wait_recv()
            for i in sends:
                self.ring(i).start()
            for place in pushes:
                self.push(place).start()

        def from_partner(self, *places):
            for place in places:
                self.push_arrival(place).wait_recv()

        def drain(self):
            for i in range(len(RING)):
                self.ring(i).wait_send()
            for place in PLACES:
                self.push(place).wait_send()

    kvs, gus, downs = Gather(0, kv, True), Gather(1, gu, False), Gather(2, dt, False)

    rows = gate_hbm.shape[0]
    to_gate = pltpu.make_async_copy(gate_hbm, gu.at[a, pl.ds(0, rows)], local_sem.at[0])
    to_up = pltpu.make_async_copy(up_hbm, gu.at[a, pl.ds(rows, rows)], local_sem.at[1])
    to_down = pltpu.make_async_copy(down_hbm, dt.at[a], local_sem.at[2])
    to_res = pltpu.make_async_copy(res_hbm, res.at[t], local_sem.at[3])
    to_ow = pltpu.make_async_copy(ow_hbm, ow, local_sem.at[4])
    to_res.start()
    to_gate.start()
    to_up.start()
    to_down.start()
    to_ow.start()

    barrier = pltpu.get_barrier_semaphore()
    for other in [*neighbour.values(), partner]:
        pl.semaphore_signal(barrier, inc=1, device_id=(other, t), device_id_type=MESH)
    for other in peers:
        pl.semaphore_signal(barrier, inc=1, device_id=(a, other), device_id_type=MESH)

    cosine, sine = cos_ref[...], sin_ref[...]
    lane = lax.broadcasted_iota(jnp.int32, cosine.shape, 1)
    low = lax.rem(lax.div(lane, 32), 2) == 0

    def rotated(x, gain):
        x = normalized(x.astype(jnp.float32)) * gain
        swapped = jnp.where(low, pltpu.roll(x, 96, 1), pltpu.roll(x, 32, 1))
        return x * cosine + swapped * sine

    tok = k_ref.shape[0]
    kv[0, 0:tok, :] = rotated(k_ref[...], kg_ref[...]).astype(jnp.bfloat16)
    for b in range(tok // 128):
        block = v_ref[b * 128:(b + 1) * 128, :].astype(jnp.float32)
        kv[0, tok + b * 128:tok + (b + 1) * 128, :] = block.T.astype(jnp.bfloat16)

    pl.semaphore_wait(barrier, len(neighbour) + 1 + len(peers))
    kvs.stage(1)

    def x_copy(src, dst, i, other):
        return pltpu.make_async_remote_copy(src_ref=src, dst_ref=dst, send_sem=x_send.at[i], recv_sem=x_recv.at[i],
                                            device_id=(a, other), device_id_type=MESH)

    def res_copy(d):
        return x_copy(res.at[t], res.at[t], d - 1, lax.rem(t + d, tp))

    def att_copy(block, d):
        return x_copy(att.at[block, t], att.at[block, t], 3 + block * 3 + d - 1, lax.rem(t + d, tp))

    def part_copy(column, d):
        other = lax.rem(t + d, tp)
        return x_copy(part.at[column, other], recv.at[column, d - 1], 15 + column * 3 + d - 1, other)

    def x_arrival(dst, i):
        return x_copy(dst, dst, i, lax.rem(t + 1, tp))

    to_res.wait()
    for d in range(1, tp):
        res_copy(d).start()

    heads = q_ref.shape[1] // 128
    blocks = tok // 128
    for h in range(heads):
        rot = rotated(q_ref[:, h * 128:(h + 1) * 128], qg_ref[...]).astype(jnp.bfloat16)
        scaled = rot.astype(jnp.float32) * LOG2_SCALE
        for b in range(blocks):
            turned = scaled[b * 128:(b + 1) * 128, :].T
            high = turned.astype(jnp.bfloat16)
            at = (b * heads + h) * 128
            qt[0:128, at:at + 128] = high
            qt[128:256, at:at + 128] = (turned - high.astype(jnp.float32)).astype(jnp.bfloat16)

    m_ref[...] = jnp.full_like(m_ref, -1e30)
    l_ref[...] = jnp.zeros_like(l_ref)
    acc[...] = jnp.zeros_like(acc)
    buffers = [s0, s1]

    def columns(j):
        return pl.ds(pl.multiple_of(j * UNIT, UNIT), UNIT)

    def score(chunk, j, into):
        keys = kv[pl.ds(chunk * 2, 2), 0:tok, :].reshape(2 * tok, 128)
        into[...] = jnp.dot(jnp.concatenate([keys, keys], axis=1), qt[:, columns(j)], preferred_element_type=jnp.float32)

    def absorb(chunk, j, held):
        turned = jnp.concatenate(
            [kv[chunk * 2 + h, tok + b * 128:tok + (b + 1) * 128, :] for h in range(2) for b in range(blocks)], axis=1)
        at = columns(j)
        scores = held[...]
        before = m_ref[:, at]
        highest = jnp.maximum(before, jnp.max(scores, axis=0, keepdims=True))
        weights = jnp.exp2(scores - highest)
        factor = jnp.exp2(before - highest)
        m_ref[:, at] = highest
        l_ref[:, at] = l_ref[:, at] * factor + jnp.sum(weights, axis=0, keepdims=True)
        acc[:, at] = acc[:, at] * factor + jnp.dot(turned, weights.astype(jnp.bfloat16), preferred_element_type=jnp.float32)

    def weights_start():
        to_gate.wait()
        to_up.wait()
        gus.stage(1)

    def downs_start():
        to_down.wait()
        downs.stage(1)

    events = {
        0: [lambda: kvs.stage(2), weights_start],
        2: [lambda: kvs.from_partner((-1, 0), (1, 0))],
        3: [lambda: kvs.from_partner((0, -1), (0, 1))],
        4: [lambda: kvs.stage(3)],
        7: [lambda: kvs.from_partner((2, 0), (0, 2))],
        8: [lambda: kvs.from_partner((-1, -1), (-1, 1)), lambda: kvs.stage(4)],
        9: [lambda: kvs.from_partner((1, -1), (1, 1)), lambda: gus.stage(2)],
    }
    kvs.from_partner((0, 0))
    score(0, 0, s0)
    n_units = blocks * heads * 128 // UNIT

    def first_phase(k, carry):
        for j in range(n_units):
            if j + 1 < n_units:
                score(k, j + 1, buffers[(j + 1) % 2])
            else:
                for at, todo in events.items():
                    @pl.when(k == at)
                    def _():
                        for event in todo:
                            event()
                score(k + 1, 0, buffers[0])
            absorb(k, j, buffers[j % 2])
        return carry

    lax.fori_loop(0, PHASE1, first_phase, 0)

    last = kv.shape[0] // 2
    before_chunk = {
        13: [lambda: kvs.from_partner((2, -1), (2, 1))],
        14: [lambda: kvs.stage(5), lambda: kvs.from_partner((-1, 2), (1, 2))],
        15: [lambda: kvs.from_partner((2, 2))],
    }
    after_tile = {0: [downs_start], 2: [lambda: gus.stage(3)], 3: [lambda: downs.stage(2)]}

    def second_phase(j, carry):
        for k in range(PHASE1, last):
            i = k - PHASE1
            if k + 1 < last:
                if k + 1 in before_chunk:
                    @pl.when(j == 0)
                    def _():
                        for event in before_chunk[k + 1]:
                            event()
                score(k + 1, j, buffers[(i + 1) % 2])
            else:
                score(PHASE1, lax.rem(j + 1, n_units), buffers[(i + 1) % 2])
            absorb(k, j, buffers[i % 2])
        at = columns(j)
        mixed = acc[:, at] / l_ref[:, at]
        for h in range(heads):
            att[j, t, :, h * 128:(h + 1) * 128] = mixed[:, h * 128:(h + 1) * 128].T.astype(jnp.bfloat16)
        for tile, todo in after_tile.items():
            @pl.when(j == tile)
            def _():
                for event in todo:
                    event()
        for d in range(1, tp):
            att_copy(j, d).start()
        return carry

    lax.fori_loop(0, n_units, second_phase, 0)

    to_ow.wait()
    for d in range(1, tp):
        x_arrival(res.at[lax.rem(t + d, tp)], tp - d - 1).wait_recv()

    after_block = {2: [lambda: gus.stage(4)], 3: [lambda: downs.stage(3)]}

    def project(b, carry):
        for d in range(1, tp):
            x_arrival(att.at[b, lax.rem(t + d, tp)], 3 + b * 3 + tp - d - 1).wait_recv()
        rows_in = jnp.concatenate([att[b, s] for s in range(tp)], axis=1)

        def column_block(i, inner):
            at = pl.ds(pl.multiple_of(i * 256, 256), 256)
            proj[:, at] = jnp.dot(rows_in, ow[:, at], preferred_element_type=jnp.float32)
            return inner

        lax.fori_loop(0, ow.shape[1] // 256, column_block, 0)

        def row_block(i, inner):
            at = pl.ds(pl.multiple_of(i * 16, 16), 16)
            stream = (res[b, at, :].astype(jnp.float32) + og_ref[...] * normalized(proj[at, :])).astype(jnp.bfloat16)
            mid[b, at, :] = stream
            nrm[pl.ds(pl.multiple_of(b * 128 + i * 16, 16), 16), :] = (mg_ref[...] * normalized(stream.astype(jnp.float32))).astype(jnp.bfloat16)
            return inner

        lax.fori_loop(0, 8, row_block, 0)
        for block, todo in after_block.items():
            @pl.when(b == block)
            def _():
                for event in todo:
                    event()
        return carry

    lax.fori_loop(0, blocks, project, 0)

    gus.stage(5)
    gus.from_partner(*PLACES)

    def hidden_block(i, carry):
        at = pl.ds(pl.multiple_of(i * 128, 128), 128)
        width = gu.shape[0] * rows
        both = jnp.concatenate([gu[:, 0:rows, at].reshape(width, 128), gu[:, rows:2 * rows, at].reshape(width, 128)], axis=1)
        gated = jnp.dot(nrm[...], both, preferred_element_type=jnp.float32)
        gate, up = gated[:, 0:128], gated[:, 128:256]
        hid[:, at] = (gate / (1.0 + jnp.exp(-gate)) * up).astype(jnp.bfloat16)
        return carry

    lax.fori_loop(0, gu.shape[2] // 128, hidden_block, 0)

    downs.stage(4)
    downs.stage(5)
    downs.from_partner(*PLACES)
    per_block = 256 // rows
    n_columns = dt.shape[0] // per_block

    def down_block(i, carry):
        weight = dt[pl.ds(i * per_block, per_block)].reshape(256, dt.shape[2])
        share = lax.dot_general(hid[...], weight, (((1,), (1,)), ((), ())), preferred_element_type=jnp.float32).astype(jnp.bfloat16)
        for b in range(blocks):
            part[i, b] = share[b * 128:(b + 1) * 128, :]

        @pl.when(i > 0)
        def _():
            for d in range(1, tp):
                part_copy(i - 1, d).start()
        return carry

    lax.fori_loop(0, n_columns, down_block, 0)
    for d in range(1, tp):
        part_copy(n_columns - 1, d).start()

    def arrived(i, carry):
        for d in range(1, tp):
            x_arrival(recv.at[i, d - 1], 15 + i * 3 + d - 1).wait_recv()
        return carry

    lax.fori_loop(0, n_columns, arrived, 0)

    def finish(i, carry):
        at = pl.ds(pl.multiple_of(i * 16, 16), 16)
        total = []
        for k in range(n_columns):
            one = part[k, t, at, :].astype(jnp.float32)
            for d in range(tp - 1):
                one = one + recv[k, d, at, :].astype(jnp.float32)
            total.append(one)
        branch = jnp.concatenate(total, axis=1)
        out_ref[at, :] = (mid[t, at, :].astype(jnp.float32) + fg_ref[...] * normalized(branch)).astype(jnp.bfloat16)
        return carry

    lax.fori_loop(0, 8, finish, 0)

    for gather in (kvs, gus, downs):
        gather.drain()
    for d in range(1, tp):
        res_copy(d).wait_send()
        for b in range(blocks):
            att_copy(b, d).wait_send()

    def drained(i, carry):
        for d in range(1, tp):
            part_copy(i, d).wait_send()
        return carry

    lax.fori_loop(0, n_columns, drained, 0)


def on_device(queries, keys, values, q_gain, k_gain, out_weight, out_gain, residual_in, mlp_gain, gate_weight, up_weight, down_weight, final_gain):
    sp, tp = lax.axis_size("sp"), lax.axis_size("tp")
    n = math.isqrt(sp // 2)
    tok, head = keys.shape
    rows, hidden = gate_weight.shape
    width = out_weight.shape[1]
    quarter = head // 4
    freqs = 10000.0 ** (-jnp.arange(quarter, dtype=jnp.float32) / quarter)
    grid_rows = tok // GRID_W
    row_angle = (lax.axis_index("sp") * grid_rows + jnp.arange(grid_rows, dtype=jnp.int32)).astype(jnp.float32)[:, None] * freqs
    column_angle = jnp.arange(GRID_W, dtype=jnp.int32).astype(jnp.float32)[:, None] * freqs
    shape = (grid_rows, GRID_W, quarter)

    def table(function, signs):
        by_row = jnp.broadcast_to(function(row_angle)[:, None], shape)
        by_column = jnp.broadcast_to(function(column_angle)[None], shape)
        return jnp.concatenate([signs[0] * by_row, signs[1] * by_row, signs[0] * by_column, signs[1] * by_column], axis=-1).reshape(tok, head)

    blocks = tok // 128
    bf16, f32 = jnp.bfloat16, jnp.float32
    vmem = pl.BlockSpec(memory_space=pltpu.VMEM)
    anywhere = pl.BlockSpec(memory_space=pl.ANY)
    n_columns = width // 256
    q_columns = tok * queries.shape[1] // head
    return pl.pallas_call(
        functools.partial(layer_kernel, n, tp),
        out_shape=jax.ShapeDtypeStruct(residual_in.shape, bf16),
        in_specs=[vmem] * 10 + [anywhere] * 5,
        out_specs=vmem,
        scratch_shapes=[
            pltpu.VMEM((sp, 2 * tok, head), bf16),
            pltpu.VMEM((sp, 2 * rows, hidden), bf16),
            pltpu.VMEM((sp, rows, hidden), bf16),
            pltpu.VMEM(out_weight.shape, bf16),
            pltpu.VMEM((tp, *residual_in.shape), bf16),
            pltpu.VMEM((blocks, tp, 128, queries.shape[1]), bf16),
            pltpu.VMEM((blocks, 128, width), bf16),
            pltpu.VMEM((tok, width), bf16),
            pltpu.VMEM((tok, hidden), bf16),
            pltpu.VMEM((n_columns, blocks, 128, 256), bf16),
            pltpu.VMEM((n_columns, tp - 1, 128, 256), bf16),
            pltpu.VMEM((128, width), f32),
            pltpu.VMEM((2 * head, q_columns), bf16),
            pltpu.VMEM((2 * tok, UNIT), f32),
            pltpu.VMEM((2 * tok, UNIT), f32),
            pltpu.VMEM((head, q_columns), f32),
            pltpu.VMEM((1, q_columns), f32),
            pltpu.VMEM((1, q_columns), f32),
            pltpu.SemaphoreType.DMA((3 * N_COPIES,)),
            pltpu.SemaphoreType.DMA((3 * N_COPIES,)),
            pltpu.SemaphoreType.DMA((39,)),
            pltpu.SemaphoreType.DMA((39,)),
            pltpu.SemaphoreType.DMA((5,)),
        ],
        compiler_params=pltpu.CompilerParams(collective_id=0, has_side_effects=True, vmem_limit_bytes=67043328),
        name="layer",
    )(queries, keys, values, table(jnp.cos, (1.0, 1.0)), table(jnp.sin, (-1.0, 1.0)),
      q_gain[None], k_gain[None], out_gain[None], mlp_gain[None], final_gain[None],
      out_weight, residual_in, gate_weight, up_weight, down_weight.T)


def solution(mesh):
    return jax.shard_map(
        on_device,
        mesh=mesh,
        in_specs=(
            P("sp", "tp"), P("sp", "tp"), P("sp", "tp"), P(), P(), P(), P(), P(("sp", "tp"), None), P(),
            P("sp", "tp"), P("sp", "tp"), P("tp", "sp"), P(),
        ),
        out_specs=P(("sp", "tp"), None),
        check_vma=False,
    )
```

time: 407 us -> 133 us (0.33)
  matrix products: 187 us -> 0 us
  Pallas kernels: 0 us -> 128 us
  blocking collectives: 68.5 us -> 0 us
  waiting for transfers between devices: 59.1 us -> 0 us
  local copies, waits for them, and re-layouts: 44.5 us -> 2 us
  other arithmetic: 30 us -> 2.27 us
  between operations: 13.4 us -> 0.08 us
    dot_general x35 -> x0, matrix products: 187 us -> none  [the longest x16 87.1 us: step(): jnp.einsum('qcgd,kcd->cgqk', grouped, key_block, preferred_element_type=j...]
    pallas_call x0 -> x1, Pallas kernels: none -> 128 us  [on_device(): pl.pallas_call(functools.partial(layer_kernel, n, tp), out_shape=jax.Shap...]
    all_to_all x3 -> x0, blocking collectives: 68.5 us -> none  [the longest x1 27.8 us: sum_at_owner(): lax.all_to_all(pieces, axis, split_axis=0, concat_axis=0, tiled=True)]
    all_gather x3 -> x0, waiting for transfers between devices: 58.4 us -> none  [the longest x2 58.4 us: in_one_piece(): lax.all_gather(both, axis, axis=dim, tiled=True)]
    reduce_sum x21 -> x0, other arithmetic: 23.1 us -> none  [the longest x16 22 us: step(): weight_sum = weight_sum * factor + jnp.sum(exp_scores, axis=-1)]
    while x48 -> x0, local copies, waits for them, and re-layouts: 22 us -> none
    unnamed x18 -> x1, local copies, waits for them, and re-layouts: 15.4 us -> 1.88 us
    split x1 -> x0, local copies, waits for them, and re-layouts: 5.85 us -> none  [in_one_piece(): jnp.split(lax.all_gather(both, axis, axis=dim, tiled=True), ends, axis=al...]
  transfers between devices with their start and end apart: 3 -> 0, of which waited for: 1 -> 0; matrix products, arithmetic and copies ran while one was open for 55% -> 0% of each run, Pallas kernels for 0% -> 0%
where the time goes in v1:
time: 133 us
  Pallas kernels  128 us (96%)
  other arithmetic  2.27 us (2%)
  local copies, waits for them, and re-layouts  2 us (2%)
    pallas_call x1, Pallas kernels, on_device(): pl.pallas_call(functools.partial(layer_kernel, n, tp), out_shape=jax.Shap...  128 us

profile of v1, /device:TPU:1, one launch (start us, length us, event | category | flops | bytes accessed | tf_op | source)
XLA Modules:
  0.0 132.6 jit_solution(13697432938160528713)
XLA Ops:
  0.0 0.2 broadcast_multiply_fusion
  0.3 0.1 broadcast_multiply_fusion.1
  0.5 1.0 pad_maximum_fusion.1
  1.5 1.0 pad_maximum_fusion
  2.5 128.3 %layer.1 = bf16[128,2048]{1,0:T(8,128)(2,1)} custom-call(bf16[512,512]{1,0:T(8,128)(2,1)} %q_ref.1, bf16[512,128]{1,0:T(8,128)(2,1)} %k_ref.1, bf16[512,128]{1,0:T(8,128)(2,1)} %v_ref.1, f32[512,128]{1,0:T(8,128)} %bitcast.9, f32[512,128]{1,0:T(8,128)} %bitcast.8, f32[1,128]{1,0:T(1,128)} %bitcast.14, f32[1,128]{1,0:T(1,128)} %bitcast.15, ...), custom_call_target="tpu_custom_call" | custom-call | tf_op jit(solution)/shard_map/layer/pallas_call | solution.py:451
  130.8 1.9 %copy.15 = bf16[128,2048]{1,0:T(8,128)(2,1)} copy(bf16[128,2048]{1,0:T(8,128)(2,1)} %layer.1) | data formatting | bytes 1048576
  (9 shorter events, 0.1 us)

commit v2 on v1

v2 whole, which is shorter than its diff:
```python
import functools
import math

import jax
import jax.numpy as jnp
import numpy as np
from jax import lax
from jax.experimental import pallas as pl
from jax.experimental.pallas import tpu as pltpu
from jax.sharding import PartitionSpec as P

GRID_W = 64
MESH = pl.DeviceIdType.MESH
EPS = 1e-06
LOG2_SCALE = 128 ** (-0.5) * math.log2(math.e)
UNIT = 512
PHASE1 = 8

RING = [
    ("A", 1, (0, 0), None, (-1, 0)),
    ("A", -1, (0, 0), None, (1, 0)),
    ("B", 1, (0, 0), None, (0, -1)),
    ("B", -1, (0, 0), None, (0, 1)),
    ("A", 1, (-1, 0), 0, (2, 0)),
    ("A", -1, (1, 0), 1, (2, 0)),
    ("B", 1, (-1, 0), None, (-1, -1)),
    ("B", -1, (-1, 0), None, (-1, 1)),
    ("B", 1, (1, 0), None, (1, -1)),
    ("B", -1, (1, 0), None, (1, 1)),
    ("B", 1, (0, -1), 0, (0, 2)),
    ("B", -1, (0, 1), 1, (0, 2)),
    ("B", 1, (2, 0), None, (2, -1)),
    ("B", -1, (2, 0), None, (2, 1)),
    ("B", 1, (-1, -1), 0, (-1, 2)),
    ("B", -1, (-1, 1), 1, (-1, 2)),
    ("B", 1, (1, -1), 0, (1, 2)),
    ("B", -1, (1, 1), 1, (1, 2)),
    ("B", 1, (2, -1), 0, (2, 2)),
    ("B", -1, (2, 1), 1, (2, 2)),
]
PLACES = [(0, 0), (-1, 0), (1, 0), (0, -1), (0, 1), (2, 0), (0, 2), (-1, -1), (-1, 1), (1, -1), (1, 1), (2, -1), (2, 1), (-1, 2), (1, 2), (2, 2)]
STAGES = {
    "1A": (None, [0, 1], [(0, 0)]),
    "1B": (None, [2, 3], []),
    "2A": (0, [4, 5, 6, 7, 8, 9], [(-1, 0), (1, 0)]),
    "2B": (1, [10, 11], [(0, -1), (0, 1)]),
    "3": (2, [12, 13, 14, 15, 16, 17], [(2, 0), (0, 2), (-1, -1), (-1, 1), (1, -1), (1, 1)]),
    "4": (3, [18, 19], [(2, -1), (2, 1), (-1, 2), (1, 2)]),
    "5": (4, [], [(2, 2)]),
}
RING_GROUPS = [[0, 1], [2, 3], [4, 5, 6, 7, 8, 9, 10, 11], [12, 13, 14, 15, 16, 17], [18, 19]]
OWN_SLOT = {(0, 0): 0, (-1, 0): 2, (1, 0): 3, (0, -1): 6, (0, 1): 7, (2, 0): 10, (0, 2): 11, (-1, -1): 12, (-1, 1): 13, (1, -1): 14, (1, 1): 15,
            (2, -1): 22, (2, 1): 23, (-1, 2): 24, (1, 2): 25, (2, 2): 30}
PARTNER_SLOT = {(0, 0): 1, (-1, 0): 4, (1, 0): 5, (0, -1): 8, (0, 1): 9, (2, 0): 16, (0, 2): 17, (-1, -1): 18, (-1, 1): 19, (1, -1): 20, (1, 1): 21,
                (2, -1): 26, (2, 1): 27, (-1, 2): 28, (1, 2): 29, (2, 2): 31}
RING_GROUP = {i: number for number, group in enumerate(RING_GROUPS) for i in group}
RING_SHARDS = [sum(2 if RING[i][3] is None else 1 for i in group) // 2 for group in RING_GROUPS]
PUSH_GROUPS = [PLACES[0:1], PLACES[1:3], PLACES[3:5], PLACES[5:7], PLACES[7:9], PLACES[9:11], PLACES[11:13], PLACES[13:15], PLACES[15:16]]
PUSH_GROUP = {place: number for number, group in enumerate(PUSH_GROUPS) for place in group}
N_GROUPS = len(RING_SHARDS) + len(PUSH_GROUPS)
ALL_SHARDS = sum(RING_SHARDS) + len(PLACES)


def normalized(x):
    return x * lax.rsqrt(jnp.mean(x * x, axis=-1, keepdims=True) + EPS)


def layer_kernel(n, tp, q_ref, k_ref, v_ref, cos_row, cos_col, sin_row, sin_col, qg_ref, kg_ref, og_ref, mg_ref, fg_ref,
                 ow_hbm, res_hbm, gate_hbm, up_hbm, down_hbm, out_ref,
                 keys, vals, gates, ups, dt, ow, res, att, mid, nrm, hid, part, recv, proj, proj_b, qt, s0, s1, acc, m_ref, l_ref,
                 send_sem, recv_sem, x_send, x_recv, local_sem):
    a = lax.axis_index("sp")
    t = lax.axis_index("tp")
    c = lax.rem(a, 2)
    chip = lax.div(a, 2)
    z = lax.div(chip, n)
    y = lax.rem(chip, n)
    u = y * (1 - c) + z * c
    w = z * (1 - c) + y * c
    partner = a + 1 - 2 * c

    def device_at(uu, ww, cc):
        return ((ww * (1 - cc) + uu * cc) * n + uu * (1 - cc) + ww * cc) * 2 + cc

    def own_index(du, dw):
        return device_at(lax.rem(u + du + n, n), lax.rem(w + dw + n, n), c)

    def partner_index(du, dw):
        return device_at(lax.rem(w + du + n, n), lax.rem(u + dw + n, n), 1 - c)

    neighbour = {("A", 1): own_index(1, 0), ("A", -1): own_index(-1, 0), ("B", 1): own_index(0, 1), ("B", -1): own_index(0, -1)}
    peers = [lax.rem(t + d, tp) for d in range(1, tp)]

    class Gather:
        def __init__(self, number, buffer, own, given, kept):
            self.number, self.buffer, self.own, self.given, self.kept = number, buffer, own, given, kept
            self.half_rows = buffer.shape[1] // 2

        def view(self, index, half=None):
            if half is None:
                return self.buffer.at[index]
            return self.buffer.at[index, pl.ds(half * self.half_rows, self.half_rows)]

        def copy(self, src, dst, group, target):
            return pltpu.make_async_remote_copy(
                src_ref=src, dst_ref=dst, send_sem=send_sem.at[self.number], recv_sem=recv_sem.at[self.number * N_GROUPS + group],
                device_id=(target, t), device_id_type=MESH)

        def ring(self, i):
            axis, sign, source, half, landing = RING[i]
            at = self.own(source)
            to = at if self.own is own_index_of else self.own(landing)
            return self.copy(self.view(at, half), self.view(to, half), RING_GROUP[i], neighbour[axis, sign])

        def push(self, place):
            return self.copy(self.view(self.own(place)), self.view(self.given(place)), len(RING_SHARDS) + PUSH_GROUP[place], partner)

        def shards(self, count, group):
            these = self.buffer.at[pl.ds(0, count)]
            return self.copy(these, these, group, partner)

        def stage(self, name):
            group, sends, places = STAGES[name]
            if group is not None:
                self.shards(RING_SHARDS[group], group).wait_recv()
            for i in sends:
                self.ring(i).start()
            for place in places:
                self.push(place).start()

        def from_partner(self, *groups):
            for group in groups:
                self.shards(len(PUSH_GROUPS[group]), len(RING_SHARDS) + group).wait_recv()

        def drain(self):
            self.shards(ALL_SHARDS, 0).wait_send()

    def own_index_of(place):
        return own_index(*place)

    def chip_slot(place, core):
        return PLACES.index(place) * 2 + core

    by_slot = (OWN_SLOT.get, PARTNER_SLOT.get, PARTNER_SLOT.get)
    by_index = (own_index_of, own_index_of, lambda place: partner_index(*place))
    ks, vs = Gather(0, keys, *by_slot), Gather(1, vals, *by_slot)
    gs, us = Gather(2, gates, *by_index), Gather(3, ups, *by_index)
    downs = Gather(4, dt, lambda place: chip_slot(place, c), lambda place: chip_slot(place[::-1], c),
                   lambda place: chip_slot(place[::-1], 1 - c))

    rows = gate_hbm.shape[0]
    to_gate = pltpu.make_async_copy(gate_hbm, gates.at[a], local_sem.at[0])
    to_up = pltpu.make_async_copy(up_hbm, ups.at[a], local_sem.at[1])
    to_down = pltpu.make_async_copy(down_hbm, dt.at[chip_slot((0, 0), c)], local_sem.at[2])
    to_res = pltpu.make_async_copy(res_hbm, res.at[t], local_sem.at[3])
    to_ow = pltpu.make_async_copy(ow_hbm, ow, local_sem.at[4])
    to_res.start()
    to_gate.start()
    to_up.start()
    to_down.start()
    to_ow.start()

    barrier = pltpu.get_barrier_semaphore()
    for other in [*neighbour.values(), partner]:
        pl.semaphore_signal(barrier, inc=1, device_id=(other, t), device_id_type=MESH)
    for other in peers:
        pl.semaphore_signal(barrier, inc=1, device_id=(a, other), device_id_type=MESH)

    tok = k_ref.shape[0]
    grid_rows = tok // GRID_W

    def table(by_row, by_column):
        mine = by_row[pl.ds(a * grid_rows, grid_rows), :]
        return jnp.concatenate([mine[r:r + 1] + by_column[...] for r in range(grid_rows)], axis=0)

    cosine, sine = table(cos_row, cos_col), table(sin_row, sin_col)
    lane = lax.broadcasted_iota(jnp.int32, cosine.shape, 1)
    low = lax.rem(lax.div(lane, 32), 2) == 0

    def rotated(x, gain):
        x = normalized(x.astype(jnp.float32)) * gain
        swapped = jnp.where(low, pltpu.roll(x, 96, 1), pltpu.roll(x, 32, 1))
        return x * cosine + swapped * sine

    keys[0] = rotated(k_ref[...], kg_ref[...]).astype(jnp.bfloat16)
    for b in range(tok // 128):
        block = v_ref[b * 128:(b + 1) * 128, :].astype(jnp.float32)
        vals[0, b * 128:(b + 1) * 128, :] = block.T.astype(jnp.bfloat16)

    heads = q_ref.shape[1] // 128
    blocks = tok // 128
    part_rows = 128 // tp
    for h in range(heads):
        rot = rotated(q_ref[:, h * 128:(h + 1) * 128], qg_ref[...]).astype(jnp.bfloat16)
        scaled = rot.astype(jnp.float32) * LOG2_SCALE
        for b in range(blocks):
            turned = jnp.concatenate([scaled[o * 128 + b * part_rows:o * 128 + (b + 1) * part_rows] for o in range(tp)], axis=0).T
            high = turned.astype(jnp.bfloat16)
            at = (b * heads + h) * 128
            qt[0:128, at:at + 128] = high
            qt[128:256, at:at + 128] = (turned - high.astype(jnp.float32)).astype(jnp.bfloat16)

    m_ref[...] = jnp.full_like(m_ref, -1e30)
    l_ref[...] = jnp.zeros_like(l_ref)
    acc[...] = jnp.zeros_like(acc)

    pl.semaphore_wait(barrier, len(neighbour) + 1 + len(peers))
    ks.stage("1A")
    vs.stage("1A")

    def x_copy(src, dst, kind, group, other):
        return pltpu.make_async_remote_copy(src_ref=src, dst_ref=dst, send_sem=x_send.at[kind], recv_sem=x_recv.at[group],
                                            device_id=(a, other), device_id_type=MESH)

    def res_copy(d):
        return x_copy(res.at[t], res.at[t], 0, 0, lax.rem(t + d, tp))

    def att_copy(block, d):
        return x_copy(att.at[block, t], att.at[block, t], 1, 1 + block, lax.rem(t + d, tp))

    def part_copy(half, column, d):
        other = lax.rem(t + d, tp)
        return x_copy(part.at[half, column, other], recv.at[half, column, d - 1], 2 + half, 5 + half * part.shape[1] + column, other)

    def x_all(these, kind, group):
        return x_copy(these, these, kind, group, lax.rem(t + 1, tp))

    to_res.wait()
    for d in range(1, tp):
        res_copy(d).start()

    buffers = [s0, s1]

    def columns(j):
        return pl.ds(pl.multiple_of(j * UNIT, UNIT), UNIT)

    def score(chunk, j, into):
        rows_in = keys[pl.ds(chunk * 2, 2)].reshape(2 * tok, 128)
        into[...] = jnp.dot(jnp.concatenate([rows_in, rows_in], axis=1), qt[:, columns(j)], preferred_element_type=jnp.float32)

    def absorb(chunk, j, held):
        turned = jnp.concatenate(
            [vals[chunk * 2 + h, b * 128:(b + 1) * 128, :] for h in range(2) for b in range(blocks)], axis=1)
        at = columns(j)
        scores = held[...]
        before = m_ref[:, at]
        highest = jnp.maximum(before, jnp.max(scores, axis=0, keepdims=True))
        weights = jnp.exp2(scores - highest)
        factor = jnp.exp2(before - highest)
        m_ref[:, at] = highest
        l_ref[:, at] = l_ref[:, at] * factor + jnp.sum(weights, axis=0, keepdims=True)
        acc[:, at] = acc[:, at] * factor + jnp.dot(turned, weights.astype(jnp.bfloat16), preferred_element_type=jnp.float32)

    def both(*groups):
        for gather in (ks, vs):
            gather.from_partner(*groups)

    events = {
        (0, 2): [lambda: ks.stage("1B"), lambda: vs.stage("1B"), lambda: to_down.wait(), lambda: downs.stage("1A"), lambda: ks.stage("2A")],
        (1, 0): [lambda: vs.stage("2A")],
        (1, 2): [lambda: ks.stage("2B"), lambda: both(1)],
        (2, 2): [lambda: vs.stage("2B")],
        (3, 2): [lambda: both(2)],
        (4, 0): [lambda: ks.stage("3")],
        (4, 2): [lambda: vs.stage("3"), lambda: to_gate.wait(), lambda: gs.stage("1A"), lambda: gs.stage("1B")],
        (6, 2): [lambda: ks.stage("4")],
        (7, 2): [lambda: both(3), lambda: vs.stage("4"), lambda: to_up.wait(), lambda: us.stage("1A"), lambda: us.stage("1B")],
    }
    ks.from_partner(0)
    score(0, 0, s0)
    vs.from_partner(0)
    n_units = blocks * heads * 128 // UNIT

    def run(table, index, *unit):
        for at, todo in table.items():
            if at[1:] == unit:
                @pl.when(index == at[0])
                def _():
                    for event in todo:
                        event()

    def first_phase(k, carry):
        for j in range(n_units):
            if j % 2 == 0:
                run(events, k, j)
            if j + 1 < n_units:
                score(k, j + 1, buffers[(j + 1) % 2])
            else:
                score(k + 1, 0, buffers[0])
            absorb(k, j, buffers[j % 2])
        return carry

    lax.fori_loop(0, PHASE1, first_phase, 0)

    last = keys.shape[0] // 2
    later = {
        (0, 8): [lambda: both(4, 5)],
        (0, 12): [lambda: both(6, 7), lambda: gs.stage("2A"), lambda: gs.stage("2B")],
        (0, 14): [lambda: ks.stage("5"), lambda: vs.stage("5"), lambda: both(8)],
        (1, 12): [lambda: us.stage("2A"), lambda: us.stage("2B")],
        (2, 12): [lambda: gs.stage("3")],
        (3, 12): [lambda: us.stage("3"), lambda: downs.stage("1B")],
    }

    def second_phase(j, carry):
        for k in range(PHASE1, last):
            i = k - PHASE1
            if i % 2 == 0:
                run(later, j, k)
            if k + 1 < last:
                score(k + 1, j, buffers[(i + 1) % 2])
            else:
                score(PHASE1, lax.rem(j + 1, n_units), buffers[(i + 1) % 2])
            absorb(k, j, buffers[i % 2])
        at = columns(j)
        mixed = acc[:, at] / l_ref[:, at]
        for h in range(heads):
            att[j, t, :, h * 128:(h + 1) * 128] = mixed[:, h * 128:(h + 1) * 128].T.astype(jnp.bfloat16)
        for d in range(1, tp):
            att_copy(j, d).start()
        return carry

    lax.fori_loop(0, n_units, second_phase, 0)

    to_ow.wait()
    x_all(res.at[pl.ds(0, tp - 1)], 0, 0).wait_recv()


    quarters = 4
    width_part = ow.shape[1] // quarters

    def dots(b, into, i):
        rows_in = jnp.concatenate([att[b, s] for s in range(tp)], axis=1)
        at = slice(i * width_part, (i + 1) * width_part)
        into[:, at] = jnp.dot(rows_in, ow[:, at], preferred_element_type=jnp.float32)

    def norms(b, held, i):
        mine = slice(b * part_rows, (b + 1) * part_rows)
        at = slice(i * part_rows, (i + 1) * part_rows)
        stream = (res[i, mine, :].astype(jnp.float32) + og_ref[...] * normalized(held[at, :])).astype(jnp.bfloat16)
        mid[i, mine, :] = stream
        nrm[b * 128 + i * part_rows:b * 128 + (i + 1) * part_rows, :] = (
            mg_ref[...] * normalized(stream.astype(jnp.float32))).astype(jnp.bfloat16)

    half_rows = tok // 2

    projected = [proj, proj_b]

    def project(first, count, after):
        for b in range(first, first + count + 1):
            now = b < first + count
            if now:
                x_all(att.at[b, pl.ds(0, tp - 1)], 1, 1 + b).wait_recv()
            for i in range(quarters):
                if now:
                    dots(b, projected[b % 2], i)
                if b > first:
                    norms(b - 1, projected[(b - 1) % 2], i)
            for event in after.get((b,), []):
                event()

    width = gates.shape[0] * rows
    n_hidden = gates.shape[2] // 128

    def feed(half, first, last_one):
        these = slice(half * half_rows, (half + 1) * half_rows)

        def gated_dot(i, into):
            at = pl.ds(pl.multiple_of(i * 128, 128), 128)
            pair = jnp.concatenate([gates[:, :, at].reshape(width, 128), ups[:, :, at].reshape(width, 128)], axis=1)
            into[0:half_rows, 0:256] = jnp.dot(nrm[these, :], pair, preferred_element_type=jnp.float32)

        def gating(i, held):
            gate, up = held[0:half_rows, 0:128], held[0:half_rows, 128:256]
            hid[these, pl.ds(pl.multiple_of(i * 128, 128), 128)] = (gate / (1.0 + jnp.exp(-gate)) * up).astype(jnp.bfloat16)

        gated_dot(first, s0)
        pairs = (last_one - first - 1) // 2

        def hidden_pair(i, carry):
            at = first + 2 * i
            gated_dot(at + 1, s1)
            gating(at, s0)
            gated_dot(at + 2, s0)
            gating(at + 1, s1)
            return carry

        lax.fori_loop(0, pairs, hidden_pair, 0)
        at = first + 2 * pairs
        if at + 1 < last_one:
            gated_dot(at + 1, s1)
            gating(at, s0)
            gating(at + 1, s1)
        else:
            gating(at, s0)

    per_block = 256 // rows
    n_columns = dt.shape[0] // per_block
    owned = half_rows // tp

    def shrink(half, first, count, before):
        these = slice(half * half_rows, (half + 1) * half_rows)

        def down_block(i, carry):
            run(before, i)
            weight = dt[pl.ds(i * per_block, per_block)].reshape(256, dt.shape[2])
            share = lax.dot_general(hid[these, :], weight, (((1,), (1,)), ((), ())), preferred_element_type=jnp.float32).astype(jnp.bfloat16)
            for o in range(tp):
                part[half, i, o] = jnp.concatenate(
                    [share[b * 128 + o * part_rows:b * 128 + (o + 1) * part_rows] for b in range(blocks // 2)], axis=0)

            @pl.when(i > first)
            def _():
                for d in range(1, tp):
                    part_copy(half, i - 1, d).start()
            return carry

        lax.fori_loop(first, first + count, down_block, 0)
        for d in range(1, tp):
            part_copy(half, first + count - 1, d).start()

    project(0, blocks - 1, {(1,): [lambda: gs.stage("4"), lambda: us.stage("4"), lambda: downs.stage("2A")],
                            (2,): [lambda: downs.stage("2B"), lambda: gs.stage("5")]})
    us.stage("5")
    for gather in (gs, us):
        gather.from_partner(*range(len(PUSH_GROUPS)))
    feed(0, 0, n_hidden)
    downs.stage("3")
    shrink(0, 0, 5, {(0,): [lambda: downs.from_partner(0, 1, 2)], (2,): [lambda: downs.from_partner(3, 4, 5)]})
    project(blocks - 1, 1, {})
    feed(1, 0, n_hidden // 2)
    downs.stage("4")
    downs.from_partner(6, 7)
    shrink(0, 5, 2, {})
    feed(1, n_hidden // 2, n_hidden)
    downs.stage("5")
    shrink(1, 0, 7, {})
    downs.from_partner(8)
    shrink(0, 7, 1, {})
    shrink(1, 7, 1, {})

    for half, columns_of in ((0, range(7)), (1, range(7)), (0, [7]), (1, [7])):
        for i in columns_of:
            x_all(recv.at[half, i], 2, 5 + half * n_columns + i).wait_recv()
            total = part[half, i, t].astype(jnp.float32)
            for d in range(tp - 1):
                total = total + recv[half, i, d].astype(jnp.float32)
            for h in range(2):
                chip_at = lax.div(own_index(*PLACES[2 * i + h]), 2)
                proj[half * owned:(half + 1) * owned, pl.ds(pl.multiple_of(chip_at * 128, 128), 128)] = total[:, h * 128:(h + 1) * 128]

    def finish(i, carry):
        at = pl.ds(pl.multiple_of(i * 32, 32), 32)
        out_ref[at, :] = (mid[t, at, :].astype(jnp.float32) + fg_ref[...] * normalized(proj[at, :])).astype(jnp.bfloat16)
        return carry

    lax.fori_loop(0, 4, finish, 0)

    for gather in (ks, vs, gs, us, downs):
        gather.drain()
    x_all(res.at[pl.ds(0, tp - 1)], 0, 0).wait_send()
    x_all(att.at[pl.ds(0, tp - 1)], 1, 0).wait_send()
    for half in range(2):
        x_all(part.at[half, pl.ds(0, n_columns * (tp - 1) // tp)], 2 + half, 0).wait_send()


def on_device(queries, keys, values, q_gain, k_gain, out_weight, out_gain, residual_in, mlp_gain, gate_weight, up_weight, down_weight, final_gain):
    sp, tp = lax.axis_size("sp"), lax.axis_size("tp")
    n = math.isqrt(sp // 2)
    tok, head = keys.shape
    rows, hidden = gate_weight.shape
    width = out_weight.shape[1]
    quarter = head // 4
    freqs = np.float32(10000.0) ** (-np.arange(quarter, dtype=np.float32) / np.float32(quarter))

    def table(function, signs, count, low):
        angle = np.arange(count, dtype=np.float32)[:, None] * freqs
        values, empty = function(angle.astype(np.float64)).astype(np.float32), np.zeros((count, 2 * quarter), np.float32)
        turned = np.concatenate([signs[0] * values, signs[1] * values], axis=1)
        return jnp.asarray(np.concatenate([turned, empty] if low else [empty, turned], axis=1).astype(np.float32))

    tables = [table(function, signs, count, low) for function, signs in ((np.cos, (1.0, 1.0)), (np.sin, (-1.0, 1.0)))
              for count, low in ((sp * tok // GRID_W, True), (GRID_W, False))]
    blocks = tok // 128
    bf16, f32 = jnp.bfloat16, jnp.float32
    vmem = pl.BlockSpec(memory_space=pltpu.VMEM)
    anywhere = pl.BlockSpec(memory_space=pl.ANY)
    n_columns = width // 256
    q_columns = tok * queries.shape[1] // head
    return pl.pallas_call(
        functools.partial(layer_kernel, n, tp),
        out_shape=jax.ShapeDtypeStruct(residual_in.shape, bf16),
        in_specs=[vmem] * 12 + [anywhere] * 5,
        out_specs=vmem,
        scratch_shapes=[
            pltpu.VMEM((sp, tok, head), bf16),
            pltpu.VMEM((sp, tok, head), bf16),
            pltpu.VMEM((sp, rows, hidden), bf16),
            pltpu.VMEM((sp, rows, hidden), bf16),
            pltpu.VMEM((sp, rows, hidden), bf16),
            pltpu.VMEM(out_weight.shape, bf16),
            pltpu.VMEM((tp, *residual_in.shape), bf16),
            pltpu.VMEM((blocks, tp, 128, queries.shape[1]), bf16),
            pltpu.VMEM((blocks, 128, width), bf16),
            pltpu.VMEM((tok, width), bf16),
            pltpu.VMEM((tok, hidden), bf16),
            pltpu.VMEM((2, n_columns, tp, 64, 256), bf16),
            pltpu.VMEM((2, n_columns, tp - 1, 64, 256), bf16),
            pltpu.VMEM((128, width), f32),
            pltpu.VMEM((128, width), f32),
            pltpu.VMEM((2 * head, q_columns), bf16),
            pltpu.VMEM((2 * tok, UNIT), f32),
            pltpu.VMEM((2 * tok, UNIT), f32),
            pltpu.VMEM((head, q_columns), f32),
            pltpu.VMEM((1, q_columns), f32),
            pltpu.VMEM((1, q_columns), f32),
            pltpu.SemaphoreType.DMA((5,)),
            pltpu.SemaphoreType.DMA((5 * N_GROUPS,)),
            pltpu.SemaphoreType.DMA((4,)),
            pltpu.SemaphoreType.DMA((5 + 2 * n_columns,)),
            pltpu.SemaphoreType.DMA((5,)),
        ],
        compiler_params=pltpu.CompilerParams(collective_id=0, has_side_effects=True, vmem_limit_bytes=67043328),
        name="layer",
    )(queries, keys, values, *tables,
      q_gain[None], k_gain[None], out_gain[None], mlp_gain[None], final_gain[None],
      out_weight, residual_in, gate_weight, up_weight, down_weight.T)


def solution(mesh):
    return jax.shard_map(
        on_device,
        mesh=mesh,
        in_specs=(
            P("sp", "tp"), P("sp", "tp"), P("sp", "tp"), P(), P(), P(), P(), P(("sp", "tp"), None), P(),
            P("sp", "tp"), P("sp", "tp"), P("tp", "sp"), P(),
        ),
        out_specs=P(("sp", "tp"), None),
        check_vma=False,
    )
```

time: 133 us -> 108 us (0.81)
  Pallas kernels: 128 us -> 106 us
  other arithmetic: 2.27 us -> 0 us
    pallas_call x1, Pallas kernels: 128 us -> 106 us  [on_device(): pl.pallas_call(functools.partial(layer_kernel, n, tp), out_shape=jax.Shap...]
    concatenate x2 -> x0, other arithmetic: 1.94 us -> none  [table(): jnp.concatenate([signs[0] * by_row, signs[1] * by_row, signs[0] * by_colu...]
where the time goes in v2:
time: 108 us
  Pallas kernels  106 us (98%)
  local copies, waits for them, and re-layouts  1.88 us (2%)
    pallas_call x1, Pallas kernels, on_device(): pl.pallas_call(functools.partial(layer_kernel, n, tp), out_shape=jax.Shap...  106 us

profile of v2, /device:TPU:1, one launch (start us, length us, event | category | flops | bytes accessed | tf_op | source)
XLA Modules:
  0.0 107.8 jit_solution(844210550347903462)
XLA Ops:
  0.0 105.9 %layer.1 = bf16[128,2048]{1,0:T(8,128)(2,1)} custom-call(bf16[512,512]{1,0:T(8,128)(2,1)} %q_ref.1, bf16[512,128]{1,0:T(8,128)(2,1)} %k_ref.1, bf16[512,128]{1,0:T(8,128)(2,1)} %v_ref.1, f32[256,128]{1,0:T(8,128)} %constant.8.clone.cos_row, f32[64,128]{1,0:T(8,128)} %constant.9.clone.cos_col, f32[256,128]{1,0:T(8,128)} %constant.10.clone.sin_row, ...), custom_call_target="tpu_custom_call" | custom-call | tf_op jit(solution)/shard_map/layer/pallas_call | solution.py:490
  106.0 1.9 %copy.19 = bf16[128,2048]{1,0:T(8,128)(2,1)} copy(bf16[128,2048]{1,0:T(8,128)(2,1)} %layer.1) | data formatting | bytes 1048576

commit v3 on v2

--- a/solution.py
+++ b/solution.py
@@ -120,9 +120,16 @@
             return self.copy(these, these, group, partner)
 
         def stage(self, name):
-            group, sends, places = STAGES[name]
+            self.arrive(name)
+            self.pass_on(name)
+
+        def arrive(self, name):
+            group = STAGES[name][0]
             if group is not None:
                 self.shards(RING_SHARDS[group], group).wait_recv()
+
+        def pass_on(self, name):
+            _, sends, places = STAGES[name]
             for i in sends:
                 self.ring(i).start()
             for place in places:
@@ -186,6 +193,31 @@
     for b in range(tok // 128):
         block = v_ref[b * 128:(b + 1) * 128, :].astype(jnp.float32)
         vals[0, b * 128:(b + 1) * 128, :] = block.T.astype(jnp.bfloat16)
+
+    pl.semaphore_wait(barrier, len(neighbour) + 1 + len(peers))
+    ks.stage("1A")
+    vs.stage("1A")
+
+    def x_copy(src, dst, kind, group, other):
+        return pltpu.make_async_remote_copy(src_ref=src, dst_ref=dst, send_sem=x_send.at[kind], recv_sem=x_recv.at[group],
+                                            device_id=(a, other), device_id_type=MESH)
+
+    def res_copy(d):
+        return x_copy(res.at[t], res.at[t], 0, 0, lax.rem(t + d, tp))
+
+    def att_copy(block, d):
+        return x_copy(att.at[block, t], att.at[block, t], 1, 1 + block, lax.rem(t + d, tp))
+
+    def part_copy(half, column, d):
+        other = lax.rem(t + d, tp)
+        return x_copy(part.at[half, column, other], recv.at[half, column, d - 1], 2 + half, 5 + half * part.shape[1] + column, other)
+
+    def x_all(these, kind, group):
+        return x_copy(these, these, kind, group, lax.rem(t + 1, tp))
+
+    to_res.wait()
+    for d in range(1, tp):
+        res_copy(d).start()
 
     heads = q_ref.shape[1] // 128
     blocks = tok // 128
@@ -204,31 +236,6 @@
     l_ref[...] = jnp.zeros_like(l_ref)
     acc[...] = jnp.zeros_like(acc)
 
-    pl.semaphore_wait(barrier, len(neighbour) + 1 + len(peers))
-    ks.stage("1A")
-    vs.stage("1A")
-
-    def x_copy(src, dst, kind, group, other):
-        return pltpu.make_async_remote_copy(src_ref=src, dst_ref=dst, send_sem=x_send.at[kind], recv_sem=x_recv.at[group],
-                                            device_id=(a, other), device_id_type=MESH)
-
-    def res_copy(d):
-        return x_copy(res.at[t], res.at[t], 0, 0, lax.rem(t + d, tp))
-
-    def att_copy(block, d):
-        return x_copy(att.at[block, t], att.at[block, t], 1, 1 + block, lax.rem(t + d, tp))
-
-    def part_copy(half, column, d):
-        other = lax.rem(t + d, tp)
-        return x_copy(part.at[half, column, other], recv.at[half, column, d - 1], 2 + half, 5 + half * part.shape[1] + column, other)
-
-    def x_all(these, kind, group):
-        return x_copy(these, these, kind, group, lax.rem(t + 1, tp))
-
-    to_res.wait()
-    for d in range(1, tp):
-        res_copy(d).start()
-
     buffers = [s0, s1]
 
     def columns(j):
@@ -257,14 +264,15 @@
 
     events = {
         (0, 2): [lambda: ks.stage("1B"), lambda: vs.stage("1B"), lambda: to_down.wait(), lambda: downs.stage("1A"), lambda: ks.stage("2A")],
-        (1, 0): [lambda: vs.stage("2A")],
-        (1, 2): [lambda: ks.stage("2B"), lambda: both(1)],
+        (1, 0): [lambda: vs.arrive("2A")],
+        (1, 2): [lambda: ks.stage("2B"), lambda: vs.pass_on("2A"), lambda: both(1)],
         (2, 2): [lambda: vs.stage("2B")],
         (3, 2): [lambda: both(2)],
         (4, 0): [lambda: ks.stage("3")],
-        (4, 2): [lambda: vs.stage("3"), lambda: to_gate.wait(), lambda: gs.stage("1A"), lambda: gs.stage("1B")],
-        (6, 2): [lambda: ks.stage("4")],
-        (7, 2): [lambda: both(3), lambda: vs.stage("4"), lambda: to_up.wait(), lambda: us.stage("1A"), lambda: us.stage("1B")],
+        (4, 2): [lambda: vs.stage("3")],
+        (5, 2): [lambda: to_gate.wait(), lambda: gs.stage("1A")],
+        (6, 2): [lambda: ks.stage("4"), lambda: gs.stage("1B")],
+        (7, 2): [lambda: both(3)],
     }
     ks.from_partner(0)
     score(0, 0, s0)
@@ -294,12 +302,13 @@
 
     last = keys.shape[0] // 2
     later = {
-        (0, 8): [lambda: both(4, 5)],
-        (0, 12): [lambda: both(6, 7), lambda: gs.stage("2A"), lambda: gs.stage("2B")],
-        (0, 14): [lambda: ks.stage("5"), lambda: vs.stage("5"), lambda: both(8)],
+        (0, 8): [lambda: vs.stage("4"), lambda: both(4, 5), lambda: to_up.wait(), lambda: us.stage("1A"), lambda: us.stage("1B")],
+        (0, 12): [lambda: both(6, 7), lambda: ks.stage("5"), lambda: gs.stage("2A"), lambda: gs.stage("2B")],
+        (0, 14): [lambda: vs.stage("5"), lambda: both(8)],
         (1, 12): [lambda: us.stage("2A"), lambda: us.stage("2B")],
-        (2, 12): [lambda: gs.stage("3")],
-        (3, 12): [lambda: us.stage("3"), lambda: downs.stage("1B")],
+        (2, 10): [lambda: gs.stage("3")],
+        (3, 8): [lambda: us.stage("3")],
+        (3, 14): [lambda: gs.stage("4"), lambda: downs.stage("1B")],
     }
 
     def second_phase(j, carry):
@@ -419,27 +428,31 @@
         for d in range(1, tp):
             part_copy(half, first + count - 1, d).start()
 
-    project(0, blocks - 1, {(1,): [lambda: gs.stage("4"), lambda: us.stage("4"), lambda: downs.stage("2A")],
-                            (2,): [lambda: downs.stage("2B"), lambda: gs.stage("5")]})
-    us.stage("5")
+    project(0, blocks - 1, {(1,): [lambda: us.stage("4"), lambda: downs.stage("2A")],
+                        (2,): [lambda: downs.stage("2B"), lambda: gs.stage("5")],
+                        (3,): [lambda: us.stage("5")]})
     for gather in (gs, us):
         gather.from_partner(*range(len(PUSH_GROUPS)))
     feed(0, 0, n_hidden)
+    downs.from_partner(0, 1, 2)
+    shrink(0, 0, 2, {})
     downs.stage("3")
-    shrink(0, 0, 5, {(0,): [lambda: downs.from_partner(0, 1, 2)], (2,): [lambda: downs.from_partner(3, 4, 5)]})
     project(blocks - 1, 1, {})
-    feed(1, 0, n_hidden // 2)
+    downs.from_partner(3, 4, 5)
+    shrink(0, 2, 3, {})
+    feed(1, 0, n_hidden)
+    shrink(1, 0, 2, {})
     downs.stage("4")
+    shrink(1, 2, 3, {})
     downs.from_partner(6, 7)
+    downs.stage("5")
     shrink(0, 5, 2, {})
-    feed(1, n_hidden // 2, n_hidden)
-    downs.stage("5")
-    shrink(1, 0, 7, {})
+    shrink(1, 5, 2, {})
     downs.from_partner(8)
     shrink(0, 7, 1, {})
     shrink(1, 7, 1, {})
 
-    for half, columns_of in ((0, range(7)), (1, range(7)), (0, [7]), (1, [7])):
+    for half, columns_of in ((0, range(5)), (1, range(5)), (0, [5, 6]), (1, [5, 6]), (0, [7]), (1, [7])):
         for i in columns_of:
             x_all(recv.at[half, i], 2, 5 + half * n_columns + i).wait_recv()
             total = part[half, i, t].astype(jnp.float32)

time: 108 us -> 105 us (0.972)
  Pallas kernels: 106 us -> 102 us
    pallas_call x1, Pallas kernels: 106 us -> 102 us  [on_device(): pl.pallas_call(functools.partial(layer_kernel, n, tp), out_shape=jax.Shap...]
where the time goes in v3:
time: 105 us; the launch traced here: 104 us
  Pallas kernels  102 us (97%)
  local copies, waits for them, and re-layouts  1.88 us (2%)
    pallas_call x1, Pallas kernels, on_device(): pl.pallas_call(functools.partial(layer_kernel, n, tp), out_shape=jax.Shap...  102 us

profile of v3, /device:TPU:1, one launch (start us, length us, event | category | flops | bytes accessed | tf_op | source)
XLA Modules:
  0.0 103.9 jit_solution(13021440110348870181)
XLA Ops:
  0.0 102.0 %layer.1 = bf16[128,2048]{1,0:T(8,128)(2,1)} custom-call(bf16[512,512]{1,0:T(8,128)(2,1)} %q_ref.1, bf16[512,128]{1,0:T(8,128)(2,1)} %k_ref.1, bf16[512,128]{1,0:T(8,128)(2,1)} %v_ref.1, f32[256,128]{1,0:T(8,128)} %constant.8.clone.cos_row, f32[64,128]{1,0:T(8,128)} %constant.9.clone.cos_col, f32[256,128]{1,0:T(8,128)} %constant.10.clone.sin_row, ...), custom_call_target="tpu_custom_call" | custom-call | tf_op jit(solution)/shard_map/layer/pallas_call | solution.py:503
  102.0 1.9 %copy.19 = bf16[128,2048]{1,0:T(8,128)(2,1)} copy(bf16[128,2048]{1,0:T(8,128)(2,1)} %layer.1) | data formatting | bytes 1048576

commit v4 on v3

--- a/solution.py
+++ b/solution.py
@@ -90,6 +90,7 @@
 
     neighbour = {("A", 1): own_index(1, 0), ("A", -1): own_index(-1, 0), ("B", 1): own_index(0, 1), ("B", -1): own_index(0, -1)}
     peers = [lax.rem(t + d, tp) for d in range(1, tp)]
+    far_first = sorted(range(1, tp), key=lambda d: -min(d, tp - d))
 
     class Gather:
         def __init__(self, number, buffer, own, given, kept):
@@ -268,10 +269,10 @@
         (1, 2): [lambda: ks.stage("2B"), lambda: vs.pass_on("2A"), lambda: both(1)],
         (2, 2): [lambda: vs.stage("2B")],
         (3, 2): [lambda: both(2)],
-        (4, 0): [lambda: ks.stage("3")],
+        (4, 0): [lambda: ks.stage("3"), lambda: to_gate.wait(), lambda: gs.stage("1A")],
         (4, 2): [lambda: vs.stage("3")],
-        (5, 2): [lambda: to_gate.wait(), lambda: gs.stage("1A")],
-        (6, 2): [lambda: ks.stage("4"), lambda: gs.stage("1B")],
+        (5, 2): [lambda: gs.stage("1B")],
+        (6, 2): [lambda: ks.stage("4"), lambda: to_up.wait(), lambda: us.stage("1A")],
         (7, 2): [lambda: both(3)],
     }
     ks.from_partner(0)
@@ -302,11 +303,12 @@
 
     last = keys.shape[0] // 2
     later = {
-        (0, 8): [lambda: vs.stage("4"), lambda: both(4, 5), lambda: to_up.wait(), lambda: us.stage("1A"), lambda: us.stage("1B")],
-        (0, 12): [lambda: both(6, 7), lambda: ks.stage("5"), lambda: gs.stage("2A"), lambda: gs.stage("2B")],
+        (0, 8): [lambda: vs.stage("4"), lambda: both(4, 5), lambda: us.stage("1B")],
+        (0, 10): [lambda: gs.stage("2A"), lambda: gs.stage("2B")],
+        (0, 12): [lambda: both(6, 7), lambda: ks.stage("5")],
         (0, 14): [lambda: vs.stage("5"), lambda: both(8)],
-        (1, 12): [lambda: us.stage("2A"), lambda: us.stage("2B")],
-        (2, 10): [lambda: gs.stage("3")],
+        (1, 10): [lambda: us.stage("2A"), lambda: us.stage("2B")],
+        (2, 8): [lambda: gs.stage("3")],
         (3, 8): [lambda: us.stage("3")],
         (3, 14): [lambda: gs.stage("4"), lambda: downs.stage("1B")],
     }
@@ -325,7 +327,7 @@
         mixed = acc[:, at] / l_ref[:, at]
         for h in range(heads):
             att[j, t, :, h * 128:(h + 1) * 128] = mixed[:, h * 128:(h + 1) * 128].T.astype(jnp.bfloat16)
-        for d in range(1, tp):
+        for d in far_first:
             att_copy(j, d).start()
         return carry
 
@@ -420,15 +422,15 @@
 
             @pl.when(i > first)
             def _():
-                for d in range(1, tp):
+                for d in far_first:
                     part_copy(half, i - 1, d).start()
             return carry
 
         lax.fori_loop(first, first + count, down_block, 0)
-        for d in range(1, tp):
+        for d in far_first:
             part_copy(half, first + count - 1, d).start()
 
-    project(0, blocks - 1, {(1,): [lambda: us.stage("4"), lambda: downs.stage("2A")],
+    project(0, blocks - 1, {(0,): [lambda: us.stage("4"), lambda: downs.stage("2A")],
                         (2,): [lambda: downs.stage("2B"), lambda: gs.stage("5")],
                         (3,): [lambda: us.stage("5")]})
     for gather in (gs, us):

time: 105 us -> 104 us (level); the launches traced: 104 us -> 104 us
  no operation moved by 1% of the time
where the time goes in v4:
time: 104 us
  Pallas kernels  102 us (98%)
  local copies, waits for them, and re-layouts  1.88 us (2%)
    pallas_call x1, Pallas kernels, on_device(): pl.pallas_call(functools.partial(layer_kernel, n, tp), out_shape=jax.Shap...  102 us

profile of v4, /device:TPU:1, one launch (start us, length us, event | category | flops | bytes accessed | tf_op | source)
XLA Modules:
  0.0 103.9 jit_solution(5581417345989814414)
XLA Ops:
  0.0 102.0 %layer.1 = bf16[128,2048]{1,0:T(8,128)(2,1)} custom-call(bf16[512,512]{1,0:T(8,128)(2,1)} %q_ref.1, bf16[512,128]{1,0:T(8,128)(2,1)} %k_ref.1, bf16[512,128]{1,0:T(8,128)(2,1)} %v_ref.1, f32[256,128]{1,0:T(8,128)} %constant.8.clone.cos_row, f32[64,128]{1,0:T(8,128)} %constant.9.clone.cos_col, f32[256,128]{1,0:T(8,128)} %constant.10.clone.sin_row, ...), custom_call_target="tpu_custom_call" | custom-call | tf_op jit(solution)/shard_map/layer/pallas_call | solution.py:505
  102.0 1.9 %copy.19 = bf16[128,2048]{1,0:T(8,128)(2,1)} copy(bf16[128,2048]{1,0:T(8,128)(2,1)} %layer.1) | data formatting | bytes 1048576

commit v5 on v4

--- a/solution.py
+++ b/solution.py
@@ -90,7 +90,6 @@
 
     neighbour = {("A", 1): own_index(1, 0), ("A", -1): own_index(-1, 0), ("B", 1): own_index(0, 1), ("B", -1): own_index(0, -1)}
     peers = [lax.rem(t + d, tp) for d in range(1, tp)]
-    far_first = sorted(range(1, tp), key=lambda d: -min(d, tp - d))
 
     class Gather:
         def __init__(self, number, buffer, own, given, kept):
@@ -327,7 +326,7 @@
         mixed = acc[:, at] / l_ref[:, at]
         for h in range(heads):
             att[j, t, :, h * 128:(h + 1) * 128] = mixed[:, h * 128:(h + 1) * 128].T.astype(jnp.bfloat16)
-        for d in far_first:
+        for d in range(1, tp):
             att_copy(j, d).start()
         return carry
 
@@ -422,12 +421,12 @@
 
             @pl.when(i > first)
             def _():
-                for d in far_first:
+                for d in range(1, tp):
                     part_copy(half, i - 1, d).start()
             return carry
 
         lax.fori_loop(first, first + count, down_block, 0)
-        for d in far_first:
+        for d in range(1, tp):
             part_copy(half, first + count - 1, d).start()
 
     project(0, blocks - 1, {(0,): [lambda: us.stage("4"), lambda: downs.stage("2A")],
@@ -437,13 +436,15 @@
         gather.from_partner(*range(len(PUSH_GROUPS)))
     feed(0, 0, n_hidden)
     downs.from_partner(0, 1, 2)
-    shrink(0, 0, 2, {})
+    shrink(0, 0, 1, {})
+    shrink(0, 1, 1, {})
     downs.stage("3")
     project(blocks - 1, 1, {})
     downs.from_partner(3, 4, 5)
     shrink(0, 2, 3, {})
     feed(1, 0, n_hidden)
-    shrink(1, 0, 2, {})
+    shrink(1, 0, 1, {})
+    shrink(1, 1, 1, {})
     downs.stage("4")
     shrink(1, 2, 3, {})
     downs.from_partner(6, 7)

time: 104 us -> 104 us (level)
  no operation moved by 1% of the time
where the time goes in v5:
time: 104 us
  Pallas kernels  102 us (98%)
  local copies, waits for them, and re-layouts  1.88 us (2%)
    pallas_call x1, Pallas kernels, on_device(): pl.pallas_call(functools.partial(layer_kernel, n, tp), out_shape=jax.Shap...  102 us

profile of v5, /device:TPU:1, one launch (start us, length us, event | category | flops | bytes accessed | tf_op | source)
XLA Modules:
  0.0 104.2 jit_solution(16816869896966498278)
XLA Ops:
  0.0 102.3 %layer.1 = bf16[128,2048]{1,0:T(8,128)(2,1)} custom-call(bf16[512,512]{1,0:T(8,128)(2,1)} %q_ref.1, bf16[512,128]{1,0:T(8,128)(2,1)} %k_ref.1, bf16[512,128]{1,0:T(8,128)(2,1)} %v_ref.1, f32[256,128]{1,0:T(8,128)} %constant.8.clone.cos_row, f32[64,128]{1,0:T(8,128)} %constant.9.clone.cos_col, f32[256,128]{1,0:T(8,128)} %constant.10.clone.sin_row, ...), custom_call_target="tpu_custom_call" | custom-call | tf_op jit(solution)/shard_map/layer/pallas_call | solution.py:506
  102.3 1.9 %copy.19 = bf16[128,2048]{1,0:T(8,128)(2,1)} copy(bf16[128,2048]{1,0:T(8,128)(2,1)} %layer.1) | data formatting | bytes 1048576
